TPU v7x, 32 devices: a whole 2x2x4 slice. The times are simulated.
32 devices in a mesh: sp: 8 (over z, x), tp: 4 (over y, core).
Axes of the slice: x: 2, y: 2, z: 4, core: 2. Of those that a mesh axis runs over, the one named last changes fastest.
Arguments:
- x_in: bfloat16 [8, 3072, 2048], P('tp', 'sp'), may hold values from -13 to 13
- x_new: bfloat16 [8, 2048], P('sp'), may hold values from -6 to 6
- w_x: bfloat16 [2048, 2048], replicated, may hold values from -0.125 to 0.125
- w_b: bfloat16 [2048, 1024], replicated, may hold values from -0.125 to 0.125
- w_c: bfloat16 [2048, 1024], replicated, may hold values from -0.125 to 0.125
- w_dt: bfloat16 [2048, 32], replicated, may hold values from -0.125 to 0.125
- w_z: bfloat16 [2048, 2048], P(None, 'tp'), may hold values from -3 to 3
- conv_w: float32 [4, 4096], replicated, may hold values from -3 to 3
- conv_b: float32 [4096], replicated, may hold values from -3 to 3
- dt_bias: float32 [32], replicated, may hold values from -4 to -2
- a_log: float32 [32], replicated, may hold values from -12 to 0
- d_skip: float32 [32], replicated, may hold values from 1 to 8
- norm_g: float32 [32, 64], P('tp'), may hold values from 0.1 to 1.9
Outputs:
- state_cache: bfloat16 [8, 32, 64, 128], P('sp', 'tp')
- read_out: bfloat16 [8, 32, 64], P('sp', 'tp')
All inputs are finite; a program needn't handle non-finite values.
Results may differ from a plain program's by a relative error of at most 0.015.
Values may be sent and summed in bfloat16 or wider, within the bound.
A program may use at most 128 MiB of HBM per device.

v0:
```python
import jax
import jax.numpy as jnp
from jax import lax
from jax.sharding import PartitionSpec as P

H = 32
P_SIZE = 64
G = 8
N = 128
KW = 4
R = 4


eps = 1e-05


def carried_in(value, axis, combine, identity):
    devices, index = (lax.axis_size(axis), lax.axis_index(axis))
    everything = lax.all_gather(value, axis)
    start = jnp.broadcast_to(jnp.asarray(identity, value.dtype), value.shape)

    def step(k, before):
        at = devices - 1 - k
        reached = at > index
        new = combine(before, everything[at])
        return jnp.where(reached, new, before)

    return lax.fori_loop(0, devices, step, start)


def passed_along(value, axis, steps):
    count = lax.axis_size(axis)
    first, last = (max(0, -steps), min(count, count - steps))
    return lax.ppermute(value, axis, [(source, source + steps) for source in range(first, last)])


def broadcast(value, axis, source):
    kept = jnp.where(lax.axis_index(axis) == source, value, 0).astype(value.dtype)
    return lax.psum(kept, axis)


def shift_conv(padded, weights, biases, col_count):
    acc_sum = biases + jnp.zeros(padded.shape[:1] + (col_count,) + padded.shape[2:], jnp.float32)
    for offset in range(KW):
        acc_sum = acc_sum + weights[offset] * padded[:, offset : offset + col_count].astype(
            jnp.float32
        )
    return jax.nn.silu(acc_sum).astype(jnp.bfloat16)


def project(token_rows, weight):
    flat_rows = token_rows.reshape(-1, token_rows.shape[-1])
    result = jnp.dot(flat_rows, weight, preferred_element_type=jnp.float32).astype(jnp.bfloat16)
    return result.reshape(token_rows.shape[:-1] + (weight.shape[1],))


def add_totals(earlier, later_part):
    return earlier + later_part


def decayed(step_sizes, rates, values, head_count):
    rest_sum = lax.cumsum(step_sizes, axis=1, reverse=True) - step_sizes
    totals = jnp.sum(step_sizes, axis=1)
    later_sum = carried_in(totals, "sp", add_totals, jnp.zeros_like(totals))
    weight = jnp.exp(rates * (rest_sum + later_sum[:, None, :])) * step_sizes
    shaped = values.astype(jnp.float32).reshape(
        values.shape[0], values.shape[1], head_count, P_SIZE
    )
    return (weight[..., None] * shaped).astype(jnp.bfloat16)


def per_device(
    x_in, x_new, w_x, w_b, w_c, w_dt, w_z, conv_w, conv_b, dt_bias, a_log, d_skip, norm_g
):
    span_len = x_in.shape[1]
    tp_size = lax.axis_size("tp")
    sp_size = lax.axis_size("sp")
    tp_rank = lax.axis_index("tp")
    sp_rank = lax.axis_index("sp")
    heads_local = H // tp_size
    groups_local = G // tp_size
    inner_cols = H * P_SIZE
    state_cols = G * N
    edge_rows = KW - 1
    decay_rates = -jnp.exp(a_log)
    bias_local = lax.dynamic_slice_in_dim(dt_bias, tp_rank * heads_local, heads_local)
    rate_local = lax.dynamic_slice_in_dim(decay_rates, tp_rank * heads_local, heads_local)
    pre_values = project(x_in, w_x)
    pre_keys = project(x_in, w_b)
    raw_steps = project(x_in, w_dt)
    pre_query = project(x_in[:, span_len - edge_rows :], w_c)
    joined = jnp.concatenate([pre_values, pre_keys], axis=2)
    before = passed_along(joined[:, span_len - edge_rows :], "sp", 1)
    conved = shift_conv(
        jnp.concatenate([before, joined], axis=1),
        conv_w[:, : inner_cols + state_cols],
        conv_b[: inner_cols + state_cols],
        span_len,
    )
    tail_rows = jnp.concatenate([joined[:, span_len - edge_rows :], pre_query], axis=2)
    last_rows = broadcast(tail_rows, "sp", sp_size - 1)
    all_tails = lax.all_gather(last_rows, "tp", axis=0, tiled=True)
    values, key_rows, raw_local = (
        lax.all_to_all(conved[..., :inner_cols], "tp", split_axis=2, concat_axis=0, tiled=True),
        lax.all_to_all(conved[..., inner_cols:], "tp", split_axis=2, concat_axis=0, tiled=True),
        lax.all_to_all(raw_steps, "tp", split_axis=2, concat_axis=0, tiled=True),
    )
    all_seqs = values.shape[0]
    step_sizes = jax.nn.softplus(raw_local.astype(jnp.float32) + bias_local)
    scaled = decayed(step_sizes, rate_local, values, heads_local)
    term_rows = jnp.einsum(
        "slgrp,slgn->sgrpn",
        scaled.reshape(all_seqs, span_len, groups_local, R, P_SIZE),
        key_rows.reshape(all_seqs, span_len, groups_local, N),
        preferred_element_type=jnp.float32,
    ).reshape(all_seqs, heads_local, P_SIZE, N)
    state_piece = lax.psum_scatter(
        term_rows.astype(jnp.bfloat16), "sp", scatter_dimension=0, tiled=True
    ).astype(jnp.float32)
    state_cache = state_piece.astype(jnp.bfloat16)
    seq_local = state_piece.shape[0]
    tails_local = lax.dynamic_slice_in_dim(all_tails, sp_rank * seq_local, seq_local, 0)
    value_cols = tp_rank * heads_local * P_SIZE
    group_cols = tp_rank * groups_local * N
    new_values = jnp.dot(
        x_new,
        lax.dynamic_slice_in_dim(w_x, value_cols, heads_local * P_SIZE, 1),
        preferred_element_type=jnp.float32,
    ).astype(jnp.bfloat16)
    new_keys = jnp.dot(
        x_new,
        lax.dynamic_slice_in_dim(w_b, group_cols, groups_local * N, 1),
        preferred_element_type=jnp.float32,
    ).astype(jnp.bfloat16)
    new_query = jnp.dot(
        x_new,
        lax.dynamic_slice_in_dim(w_c, group_cols, groups_local * N, 1),
        preferred_element_type=jnp.float32,
    ).astype(jnp.bfloat16)
    new_raw = jnp.dot(
        x_new,
        lax.dynamic_slice_in_dim(w_dt, tp_rank * heads_local, heads_local, 1),
        preferred_element_type=jnp.float32,
    ).astype(jnp.bfloat16)
    gate_new = jnp.dot(x_new, w_z, preferred_element_type=jnp.float32).astype(jnp.bfloat16)

    def new_conv(newest, col_start, col_count):
        history = lax.dynamic_slice_in_dim(tails_local, col_start, col_count, 2)
        padded = jnp.concatenate([history, newest[:, None, :]], axis=1)
        return shift_conv(
            padded,
            lax.dynamic_slice_in_dim(conv_w, col_start, col_count, 1),
            lax.dynamic_slice_in_dim(conv_b, col_start, col_count, 0),
            1,
        )[:, 0]

    conv_values = new_conv(new_values, value_cols, heads_local * P_SIZE)
    value_rows = conv_values.astype(jnp.float32).reshape(seq_local, groups_local, R, P_SIZE)
    conv_keys = new_conv(new_keys, inner_cols + group_cols, groups_local * N)
    conv_keys = conv_keys.astype(jnp.float32).reshape(seq_local, groups_local, N)
    conv_query = new_conv(new_query, inner_cols + state_cols + group_cols, groups_local * N)
    conv_query = conv_query.astype(jnp.float32).reshape(seq_local, groups_local, N)
    new_steps = jax.nn.softplus(new_raw.astype(jnp.float32) + bias_local)
    decay_new = jnp.exp(rate_local * new_steps).reshape(seq_local, groups_local, R)
    held_read = jnp.einsum(
        "sgrpn,sgn->sgrp",
        state_piece.reshape(seq_local, groups_local, R, P_SIZE, N),
        conv_query,
        precision=lax.Precision.HIGHEST,
    )
    inner_prod = jnp.sum(conv_query * conv_keys, axis=-1)
    step_group = new_steps.reshape(seq_local, groups_local, R)
    skip_local = lax.dynamic_slice_in_dim(d_skip, tp_rank * heads_local, heads_local).reshape(
        groups_local, R
    )
    output = (
        decay_new[..., None] * held_read
        + (step_group * inner_prod[:, :, None])[..., None] * value_rows
        + skip_local[None, :, :, None] * value_rows
    )
    gate_rows = gate_new.astype(jnp.float32).reshape(seq_local, groups_local, R, P_SIZE)
    gated_out = output * jax.nn.silu(gate_rows)
    group_ms = jnp.mean(gated_out * gated_out, axis=(2, 3))
    read_out = (
        gated_out
        * lax.rsqrt(group_ms + eps)[:, :, None, None]
        * norm_g.reshape(groups_local, R, P_SIZE)
    )
    read_out = read_out.astype(jnp.bfloat16).reshape(seq_local, heads_local, P_SIZE)
    return (state_cache, read_out)


def solution(mesh):
    return jax.shard_map(
        per_device,
        mesh=mesh,
        in_specs=(
            P("tp", "sp", None),
            P("sp", None),
            P(),
            P(),
            P(),
            P(),
            P(None, "tp"),
            P(),
            P(),
            P(),
            P(),
            P(),
            P("tp", None),
        ),
        out_specs=(P("sp", "tp", None, None), P("sp", "tp", None)),
        check_vma=False,
    )
```

profile of v0, /device:TPU:5, one launch (start us, length us, event | category | flops | bytes accessed | tf_op | source)
XLA Modules:
  0.0 254.8 jit_solution(16243025266808292182)
XLA Ops:
  7.2 6.7 %convolution_convert_fusion.1 = bf16[768,1024]{1,0:T(8,128)(2,1)S(1)} fusion(bf16[768,2048]{1,0:T(8,128)(2,1)} %bitcast.211, bf16[2048,1024]{1,0:T(8,128)(2,1)} %param.18), kind=kOutput, calls=%fused_computation.13 | convolution fusion | flops 3222011904 | bytes 8912896 | tf_op jit(solution)/shard_map/dot_general | solution.py:53
  13.9 6.9 %convolution_convert_fusion = bf16[768,2048]{1,0:T(8,128)(2,1)S(1)} fusion(bf16[768,2048]{1,0:T(8,128)(2,1)S(1)} %bitcast.212, bf16[2048,2048]{1,0:T(8,128)(2,1)S(1)} %copy-done.9), kind=kOutput, calls=%fused_computation.8 | convolution fusion | flops 6444023808 | bytes 14680064 | tf_op jit(solution)/shard_map/dot_general | solution.py:53
  20.8 1.6 copy-done.2
  22.5 3.1 %collective-permute-start = (bf16[2,3,3072]{2,0,1:T(2,128)(2,1)S(1)}, bf16[2,3,3072]{2,0,1:T(2,128)(2,1)S(1)}, u32[]{:S(2)}, u32[]{:S(2)}) collective-permute-start(bf16[2,3,3072]{2,0,1:T(2,128)(2,1)S(1)} %copy.90), channel_id=1, source_target_pairs={{0,4},{4,8},{8,12},{12,16},{16,20},{20,24},{24,28},{1,5},{5,9},{9,... | collective-permute-start | bytes 110600 | tf_op jit(solution)/shard_map/ppermute | solution.py:34
  27.4 4.3 %all-to-all-start = ((bf16[2,384,32]{1,0,2:T(2,128)(2,1)}), bf16[2,384,32]{1,0,2:T(2,128)(2,1)S(1)}, u32[]{:S(2)}, u32[]{:S(2)}) async-start(bf16[2,384,32]{1,0,2:T(2,128)(2,1)} %reshape.271), calls=%async_computation | async-start | bytes 98304 | tf_op jit(solution)/shard_map/all_to_all | solution.py:106
  32.6 2.8 %convolution_convert_fusion.3 = bf16[6,1024]{1,0:T(8,128)(2,1)S(1)} fusion(bf16[6,2048]{1,0:T(8,128)(2,1)S(1)} %reshape.279, bf16[2048,1024]{1,0:T(8,128)(2,1)} %param.19), kind=kOutput, calls=%fused_computation.16 | convolution fusion | flops 25171968 | bytes 4231168 | tf_op jit(solution)/shard_map/dot_general | solution.py:53
  36.4 3.5 %maximum_maximum_fusion = bf16[2,387,3072]{2,1,0:T(8,128)(2,1)S(1)} fusion(bf16[2,384,1024]{2,1,0:T(8,128)(2,1)} %bitcast.209, bf16[2,384,2048]{2,1,0:T(8,128)(2,1)} %bitcast.205, bf16[2,3,3072]{2,1,0:T(4,128)(2,1)S(1)} %copy.91), kind=kLoop, calls=%fused_computation.7 | loop fusion | flops 14266368 | bytes 9510912 | tf_op jit(solution)/shard_map/concatenate | solution.py:95
  40.1 7.3 %multiply_convert_fusion = bf16[2,384,3072]{2,1,0:T(8,128)(2,1)S(1)} fusion(bf16[2,384,1024]{2,1,0:T(8,128)(2,1)S(1)} %bitcast.210, bf16[2,384,2048]{2,1,0:T(8,128)(2,1)S(1)} %bitcast.206, bf16[2,387,3072]{2,1,0:T(8,128)(2,1)S(1)} %maximum_maximum_fusion, f32[3072]{0:T(1024)S(1)} %bitcast.221, f32[3072]{0:T(1024)S(1)} %bitcast.222, f32[3072]{0:T(1024)S(1)} %bitcast.223, ...), kind=kLoop, calls=%fused_computation.1 | loop fusion | flops 47185920 | bytes 23654400 | tf_op jit(solution)/shard_map/convert_element_type | solution.py:48
  47.4 2.1 copy-done.4
  49.6 3.1 %copy.94 = bf16[2,384,1024]{1,0,2:T(2,128)(2,1)} copy(bf16[2,384,1024]{2,1,0:T(8,128)(2,1)S(1)} %slice.154) | data formatting | bytes 3145728 | tf_op jit(solution)/shard_map/slice | solution.py:105
  52.7 3.6 %all-to-all-start.2 = ((bf16[2,384,1024]{1,0,2:T(2,128)(2,1)}), bf16[2,384,1024]{1,0,2:T(2,128)(2,1)S(1)}, u32[]{:S(2)}, u32[]{:S(2)}) async-start(bf16[2,384,1024]{1,0,2:T(2,128)(2,1)} %copy.94), calls=%async_computation.2 | async-start | bytes 3145728 | tf_op jit(solution)/shard_map/all_to_all | solution.py:105
  56.5 28.5 %psum.7 = bf16[2,3,4096]{2,1,0:T(4,128)(2,1)S(1)} all-reduce(bf16[2,3,4096]{2,1,0:T(4,128)(2,1)S(1)} %maximum_select_fusion), channel_id=1, replica_groups=mesh['sp'=8,'tp'=4] {'sp'}, use_global_device_ids=true, to_apply=%region_6.7 | all-reduce | flops 24576 | bytes 98304 | tf_op jit(solution)/shard_map/psum | solution.py:39
  85.1 13.2 %all_gather.11 = bf16[8,3,4096]{2,1,0:T(4,128)(2,1)S(1)} all-gather(bf16[2,3,4096]{2,1,0:T(4,128)(2,1)S(1)} %psum.7), channel_id=1, replica_groups=mesh['sp'=8,'tp'=4] {'tp'}, dimensions={0}, use_global_device_ids=true | all-gather | bytes 245760 | tf_op jit(solution)/shard_map/all_gather | solution.py:102
  98.4 3.9 %slice.153 = bf16[2,384,2048]{2,1,0:T(8,128)(2,1)} slice(bf16[2,384,3072]{2,1,0:T(8,128)(2,1)} %copy-done.4), slice={[0:2], [0:384], [0:2048]} | slice | bytes 6291456 | tf_op jit(solution)/shard_map/slice | solution.py:104
  102.3 8.8 %copy.92 = bf16[2,384,2048]{1,0,2:T(2,128)(2,1)} copy(bf16[2,384,2048]{2,1,0:T(8,128)(2,1)} %slice.153) | data formatting | bytes 6291456 | tf_op jit(solution)/shard_map/slice | solution.py:104
  111.2 4.9 %all-to-all-start.1 = ((bf16[2,384,2048]{1,0,2:T(2,128)(2,1)}), bf16[2,384,2048]{1,0,2:T(2,128)(2,1)}, u32[]{:S(2)}, u32[]{:S(2)}) async-start(bf16[2,384,2048]{1,0,2:T(2,128)(2,1)} %copy.92), calls=%async_computation.1 | async-start | bytes 6291456 | tf_op jit(solution)/shard_map/all_to_all | solution.py:104
  116.4 29.7 %reduce-window.6 = f32[8,8,3,128]{3,1,2,0:T(8,128)S(1)} reduce-window(f32[8,8,3,128]{3,1,2,0:T(8,128)S(1)} %bitcast.218, f32[]{:T(128)} %constant.133.clone.1), window={size=1x1x1x128 pad=0_0x0_0x0_0x0_127}, to_apply=%region_0.1 | reduce-window | flops 3121152 | bytes 196612 | tf_op jit(solution)/shard_map/reduce-window
  146.4 24.2 %all_gather.10 = f32[8,8,8]{2,1,0:T(8,128)S(1)} all-gather(f32[1,8,8]{2,1,0:T(8,128)S(1)} %bitcast.225), channel_id=1, replica_groups=mesh['sp'=8,'tp'=4] {'sp'}, dimensions={0}, use_global_device_ids=true | all-gather | bytes 2304 | tf_op jit(solution)/shard_map/all_gather | solution.py:19
  172.6 4.0 %convert_bitcast_fusion = f32[4,2,384,512]{2,1,3,0:T(2,128)S(1)} fusion(bf16[2,384,4,512]{1,0,3,2:T(2,128)(2,1)} %bitcast.59), kind=kLoop, calls=%fused_computation.2 | loop fusion | flops 1572864 | bytes 9437184 | tf_op jit(solution)/shard_map/convert_element_type | solution.py:66
  178.1 2.0 fusion.4
  180.1 2.0 fusion.2
  182.7 1.5 fusion.8
  184.1 1.5 fusion.10
  186.0 60.0 %reduce-scatter.2.cloned.1.call-done = bf16[1,8,64,128]{3,2,1,0:T(8,128)(2,1)} async-done(((bf16[8,8,64,128]{3,2,1,0:T(8,128)(2,1)}), bf16[1,8,64,128]{3,2,1,0:T(8,128)(2,1)}) %reduce-scatter.2.cloned.1.call-update) | async-done | bytes 131088 | tf_op jit(solution)/shard_map/reduce_scatter | solution.py:117
  (106 shorter events, 11.2 us)
Async XLA Ops:
  7.2 28.3 %copy-start = (bf16[2048,512]{1,0:T(8,128)(2,1)S(1)}, bf16[2048,512]{1,0:T(8,128)(2,1)}, u32[]{:S(2)}) copy-start(bf16[2048,512]{1,0:T(8,128)(2,1)} %param.21) | copy-start | bytes 6291460
  7.2 6.7 %copy-start.7 = (bf16[2,384,2048]{2,1,0:T(8,128)(2,1)S(1)}, bf16[2,384,2048]{2,1,0:T(8,128)(2,1)}, u32[]{:S(2)}) copy-start(bf16[2,384,2048]{2,1,0:T(8,128)(2,1)} %param.15) | copy-start | bytes 9437188
  7.2 6.7 %copy-start.9 = (bf16[2048,2048]{1,0:T(8,128)(2,1)S(1)}, bf16[2048,2048]{1,0:T(8,128)(2,1)}, u32[]{:S(2)}) copy-start(bf16[2048,2048]{1,0:T(8,128)(2,1)} %param.17) | copy-start | bytes 25165828
  13.9 6.9 %copy-start.5 = (bf16[768,1024]{1,0:T(8,128)(2,1)}, bf16[768,1024]{1,0:T(8,128)(2,1)S(1)}, u32[]{:S(2)}) copy-start(bf16[768,1024]{1,0:T(8,128)(2,1)S(1)} %convolution_convert_fusion.1) | copy-start | bytes 4718596
  20.8 1.6 copy-start.2
  20.8 4.8 %copy-start.11 = (bf16[2048,32]{0,1:T(8,128)(2,1)S(1)}, bf16[2048,32]{0,1:T(8,128)(2,1)}, u32[]{:S(2)}) copy-start(bf16[2048,32]{0,1:T(8,128)(2,1)} %param.20) | copy-start | bytes 393220
  22.4 10.1 %copy-start.12 = (f32[4,4096]{1,0:T(4,128)S(1)}, f32[4,4096]{1,0:T(4,128)}, u32[]{:S(2)}) copy-start(f32[4,4096]{1,0:T(4,128)} %param.22) | copy-start | bytes 196612
  22.5 13.0 %copy-start.10 = (bf16[1,2048]{1,0:T(2,128)(2,1)S(1)}, bf16[1,2048]{1,0:T(2,128)(2,1)}, u32[]{:S(2)}) copy-start(bf16[1,2048]{1,0:T(2,128)(2,1)} %param.16) | copy-start | bytes 12292
  22.5 13.8 %collective-permute-start = (bf16[2,3,3072]{2,0,1:T(2,128)(2,1)S(1)}, bf16[2,3,3072]{2,0,1:T(2,128)(2,1)S(1)}, u32[]{:S(2)}, u32[]{:S(2)}) collective-permute-start(bf16[2,3,3072]{2,0,1:T(2,128)(2,1)S(1)} %copy.90), channel_id=1, source_target_pairs={{0,4},{4,8},{8,12},{12,16},{16,20},{20,24},{24,28},{1,5},{5,9},{9,... | collective-permute-start | bytes 110600 | tf_op jit(solution)/shard_map/ppermute | solution.py:34
  26.7 9.4 %copy-start.13 = (f32[4096]{0:T(1024)S(1)}, f32[4096]{0:T(1024)}, u32[]{:S(2)}) copy-start(f32[4096]{0:T(1024)} %param.23) | copy-start | bytes 49156
  26.7 9.5 %copy-start.16 = (f32[32]{0:T(128)S(1)}, f32[32]{0:T(128)}, u32[]{:S(2)}) copy-start(f32[32]{0:T(128)} %param.24) | copy-start | bytes 388
  27.4 25.4 %all-to-all-start = ((bf16[2,384,32]{1,0,2:T(2,128)(2,1)}), bf16[2,384,32]{1,0,2:T(2,128)(2,1)S(1)}, u32[]{:S(2)}, u32[]{:S(2)}) async-start(bf16[2,384,32]{1,0,2:T(2,128)(2,1)} %reshape.271), calls=%async_computation | async-start | bytes 98304 | tf_op jit(solution)/shard_map/all_to_all | solution.py:106
  36.3 3.5 %copy-start.3 = (bf16[768,2048]{1,0:T(8,128)(2,1)S(1)}, bf16[768,2048]{1,0:T(8,128)(2,1)}, u32[]{:S(2)}) copy-start(bf16[768,2048]{1,0:T(8,128)(2,1)} %copy-done.2) | copy-start | bytes 9437188
  36.3 3.8 %copy-start.6 = (bf16[768,1024]{1,0:T(8,128)(2,1)S(1)}, bf16[768,1024]{1,0:T(8,128)(2,1)}, u32[]{:S(2)}) copy-start(bf16[768,1024]{1,0:T(8,128)(2,1)} %copy-done.5) | copy-start | bytes 4718596
  36.3 3.8 %slice-start = ((f32[4096]{0:T(1024)}), f32[3072]{0:T(1024)S(1)}, s32[]{:S(2)}) async-start(f32[4096]{0:T(1024)} %param.23), calls=%async_computation.5 | async-start | bytes 24576 | tf_op jit(solution)/shard_map/slice | solution.py:97
  47.4 2.1 copy-start.4
  49.5 48.8 %copy-start.17 = (f32[32]{0:T(128)S(1)}, f32[32]{0:T(128)}, u32[]{:S(2)}) copy-start(f32[32]{0:T(128)} %param.25) | copy-start | bytes 388
  52.7 58.5 %all-to-all-start.2 = ((bf16[2,384,1024]{1,0,2:T(2,128)(2,1)}), bf16[2,384,1024]{1,0,2:T(2,128)(2,1)S(1)}, u32[]{:S(2)}, u32[]{:S(2)}) async-start(bf16[2,384,1024]{1,0,2:T(2,128)(2,1)} %copy.94), calls=%async_computation.2 | async-start | bytes 3145728 | tf_op jit(solution)/shard_map/all_to_all | solution.py:105
  111.2 61.4 %all-to-all-start.1 = ((bf16[2,384,2048]{1,0,2:T(2,128)(2,1)}), bf16[2,384,2048]{1,0,2:T(2,128)(2,1)}, u32[]{:S(2)}, u32[]{:S(2)}) async-start(bf16[2,384,2048]{1,0,2:T(2,128)(2,1)} %copy.92), calls=%async_computation.1 | async-start | bytes 6291456 | tf_op jit(solution)/shard_map/all_to_all | solution.py:104
  116.1 129.9 %reduce-scatter.2.cloned.1.call-start = ((), (), s32[]{:S(2)}) async-start(), calls=%async_computation.4 | async-start | bytes 1179648 | tf_op jit(solution)/shard_map/reduce_scatter | solution.py:117
  178.1 4.2 %copy-start.18 = (f32[32]{0:T(128)S(1)}, f32[32]{0:T(128)}, u32[]{:S(2)}) copy-start(f32[32]{0:T(128)} %param.26) | copy-start | bytes 388
  178.1 4.5 %copy-start.14 = (f32[4096]{0:T(1024)S(1)}, f32[4096]{0:T(1024)}, u32[]{:S(2)}) copy-start(f32[4096]{0:T(1024)} %param.23) | copy-start | bytes 49156
  178.1 69.9 %copy-start.1 = (bf16[2048,512]{1,0:T(8,128)(2,1)S(1)}, bf16[2048,512]{1,0:T(8,128)(2,1)}, u32[]{:S(2)}) copy-start(bf16[2048,512]{1,0:T(8,128)(2,1)} %param.21) | copy-start | bytes 6291460
  180.1 67.2 %copy-start.15 = (f32[8,64]{1,0:T(8,128)S(1)}, f32[8,64]{1,0:T(8,128)}, u32[]{:S(2)}) copy-start(f32[8,64]{1,0:T(8,128)} %param.27) | copy-start | bytes 6148
  (1 other events, 1.4 us)
Sparse Core Ops, SparseCore 0:
  180.3 65.7 reduce-scatter.1
where the time goes:
time: 259 us; the launch traced here: 255 us
  blocking collectives  66 us (25%)
  waiting for transfers between devices  60 us (23%)
  other arithmetic  46.7 us (18%)
  matrix products  25.9 us (10%)
  local copies, waits for them, and re-layouts  25.7 us (10%)
  starting transfers between devices  15.9 us (6%)
  between operations  14.5 us (6%)
    reduce_scatter x1, waiting for transfers between devices, per_device(): lax.psum_scatter(term_rows.astype(jnp.bfloat16), 'sp', scatter_dimension=...  60 us
    another operation x2, other arithmetic  29.8 us
    psum x1, blocking collectives, broadcast(): return lax.psum(kept, axis)  28.5 us
    all_gather x1, blocking collectives, carried_in(): everything = lax.all_gather(value, axis)  24.2 us
    dot_general x4, matrix products, project(): jnp.dot(flat_rows, weight, preferred_element_type=jnp.float32)  17.4 us
    all_gather x1, blocking collectives, per_device(): all_tails = lax.all_gather(last_rows, 'tp', axis=0, tiled=True)  13.2 us
    slice x2, local copies, waits for them, and re-layouts, per_device(): conved[..., :inner_cols]  12.7 us
    convert_element_type x1, other arithmetic, shift_conv(): return jax.nn.silu(acc_sum).astype(jnp.bfloat16)  7.28 us
  transfers between devices with their start and end apart: 5, of which 1 were waited for; matrix products, arithmetic and copies ran while one was open for 28% of the time, Pallas kernels for 0%

commit v1 on v0

v1 whole, which is shorter than its diff:
```python
import functools

import jax
import jax.numpy as jnp
from jax import lax
from jax.experimental import pallas as pl
from jax.experimental.pallas import tpu as pltpu
from jax.sharding import PartitionSpec as P

MESH = pl.DeviceIdType.MESH
F32 = jnp.float32
BF16 = jnp.bfloat16
EPS = 1e-05
EDGE = 16
PAIR = 2
LANES = 128


def silu(x):
    half = 0.5 * x
    return half + half * jnp.tanh(half)


def softplus(x):
    return jnp.maximum(x, 0.0) + jnp.log1p(jnp.exp(-jnp.abs(x)))


def rounded(x):
    return x.astype(BF16).astype(F32)


def kernel(
    dims,
    x_ref, xn_ref, wx_ref, wb_ref, wc_ref, wdt_ref, wz_ref,
    cw_ref, cb_ref, dtb_ref, alog_ref, dskip_ref, ng_ref,
    state_ref, read_ref,
    xs, wxs, wbs, wdts, wxn, wbn, wcn, wzn, nt, pre0, pre1, padded,
    wt, tot_out, tot_in, rate_s, st_out, st_in, head_s, read_s,
    x_sem, wdt_sem, w_sem, new_sem, halo_send, halo_recv, tail_send, tail_recv,
    tot_send, tot_recv, st_send, st_recv,
):
    sp, tp, heads, groups, n_size, p_size, ratio, taps = dims
    i, j = lax.axis_index("sp"), lax.axis_index("tp")
    spt, length, _ = x_ref.shape
    hl, gl = heads // tp, groups // tp
    inner, keys_all = heads * p_size, groups * n_size
    gcols = ratio * p_size
    steps = groups // PAIR
    home = i // spt
    own = home == j
    pres = (pre0, pre1)

    barrier = pltpu.get_barrier_semaphore()
    for k in range(sp):
        @pl.when(jnp.logical_not(own & (i == k)))
        def _():
            pl.semaphore_signal(barrier, inc=1, device_id={"sp": k, "tp": home}, device_id_type=MESH)
    before, after = lax.rem(i + sp - 1, sp), lax.rem(i + 1, sp)
    pl.semaphore_signal(barrier, inc=1, device_id={"sp": before, "tp": j}, device_id_type=MESH)

    wdt_copy = pltpu.make_async_copy(wdt_ref, wdts, wdt_sem)
    x_copies = [
        pltpu.make_async_copy(x_ref.at[a], xs.at[a, pl.ds(EDGE, length)], x_sem.at[a])
        for a in range(spt)
    ]
    w_copies = []
    for s in range(steps):
        w_copies.append((
            pltpu.make_async_copy(
                wx_ref.at[:, pl.ds(s * PAIR * gcols, PAIR * gcols)], wxs.at[s], w_sem.at[s, 0]),
            pltpu.make_async_copy(
                wb_ref.at[:, pl.ds(s * PAIR * n_size, PAIR * n_size)], wbs.at[s], w_sem.at[s, 1]),
        ))
    vcol = pl.multiple_of(j * (hl * p_size), LANES)
    gcol = pl.multiple_of(j * (gl * n_size), LANES)
    new_copies = [
        pltpu.make_async_copy(wx_ref.at[:, pl.ds(vcol, hl * p_size)], wxn, new_sem.at[0]),
        pltpu.make_async_copy(wb_ref.at[:, pl.ds(gcol, gl * n_size)], wbn, new_sem.at[1]),
        pltpu.make_async_copy(wc_ref.at[:, pl.ds(gcol, gl * n_size)], wcn, new_sem.at[2]),
        pltpu.make_async_copy(wz_ref, wzn, new_sem.at[3]),
    ]
    wdt_copy.start()
    for c in x_copies:
        c.start()
    for pair in w_copies:
        for c in pair:
            c.start()
    for c in new_copies:
        c.start()

    pl.semaphore_wait(barrier, spt * tp + 1 - own.astype(jnp.int32))

    def halo(a):
        return pltpu.make_async_remote_copy(
            src_ref=x_ref.at[a, pl.ds(length - EDGE, EDGE)],
            dst_ref=xs.at[a, pl.ds(0, EDGE)],
            send_sem=halo_send.at[a], recv_sem=halo_recv.at[a],
            device_id={"sp": after, "tp": j}, device_id_type=MESH)

    for a in range(spt):
        halo(a).start()

    def is_self(a, q):
        return (spt * j + a == i) & (j == q)

    def either(a, q, remote, local):
        here = is_self(a, q)
        pl.when(jnp.logical_not(here))(remote)
        if local is not None:
            pl.when(here)(local)

    def tail(a, q):
        src, dst = x_ref.at[a, pl.ds(length - EDGE, EDGE)], nt.at[pl.ds(0, EDGE)]
        return pltpu.make_async_remote_copy(
            src_ref=src, dst_ref=dst, send_sem=tail_send.at[a, q], recv_sem=tail_recv.at[0],
            device_id={"sp": spt * j + a, "tp": q}, device_id_type=MESH
        ), pltpu.make_async_copy(src, dst, tail_recv.at[0])

    @pl.when(i == sp - 1)
    def _():
        for a in range(spt):
            for q in range(tp):
                remote, local = tail(a, q)
                either(a, q, remote.start, local.start)

    padded[...] = jnp.zeros_like(padded)
    padded[0:1, 0:heads] = alog_ref[...]
    spread = jnp.broadcast_to(padded[0:1, :], (LANES, LANES)).T[0:heads]
    rates = -jnp.exp(spread)
    for q in range(tp):
        rate_s[q] = rates[q * hl:(q + 1) * hl]
    padded[0:1, 0:heads] = jnp.zeros((1, heads), F32)

    rows = lax.broadcasted_iota(jnp.int32, (length, length), 0)
    cols = lax.broadcasted_iota(jnp.int32, (length, length), 1)
    later = (rows > cols).astype(F32).astype(BF16)
    wdt_copy.wait()

    def tot(a, q):
        src, dst = tot_out.at[a, q], tot_in.at[i]
        return pltpu.make_async_remote_copy(
            src_ref=src, dst_ref=dst, send_sem=tot_send.at[a, q], recv_sem=tot_recv.at[i],
            device_id={"sp": spt * j + a, "tp": q}, device_id_type=MESH
        ), pltpu.make_async_copy(src, dst, tot_recv.at[i])

    for a in range(spt):
        x_copies[a].wait()
        raw = jnp.dot(xs[a, EDGE:, :], wdts[...], preferred_element_type=F32)
        padded[:, 0:heads] = softplus(rounded(raw) + dtb_ref[...])
        sizes = padded[...].T[0:heads]
        rest = jnp.zeros_like(sizes)
        left = sizes
        for _ in range(3):
            term = left.astype(BF16)
            rest += jnp.dot(term, later, preferred_element_type=F32)
            left = left - term.astype(F32)
        wt[a] = jnp.exp(rates[:, 0:1] * rest) * sizes
        total = jnp.broadcast_to(rest[:, 0:1] + sizes[:, 0:1], (heads, LANES))
        for q in range(tp):
            tot_out[a, q] = total[q * hl:(q + 1) * hl]
    for a in range(spt):
        for q in range(tp):
            remote, local = tot(a, q)
            either(a, q, remote.start, local.start)

    for a in range(spt):
        halo(a).wait()
        xs[a, 0:EDGE, :] = jnp.where(i == 0, 0.0, xs[a, 0:EDGE, :].astype(F32)).astype(BF16)

    def state_copy(a, g):
        q = g // gl
        src, dst = st_out.at[a, g], st_in.at[i, lax.rem(g, gl)]
        sem = st_recv.at[i, lax.rem(g, gl)]
        return q, pltpu.make_async_remote_copy(
            src_ref=src, dst_ref=dst, send_sem=st_send.at[a, g], recv_sem=sem,
            device_id={"sp": spt * j + a, "tp": q}, device_id_type=MESH
        ), pltpu.make_async_copy(src, dst, sem)

    vtiles, ktiles = PAIR * gcols // LANES, PAIR * n_size // LANES
    tiles_group = gcols // LANES
    heads_tile = LANES // p_size

    def step(s, carry):
        pltpu.make_async_copy(wx_ref.at[:, pl.ds(0, PAIR * gcols)], wxs.at[s], w_sem.at[s, 0]).wait()
        pltpu.make_async_copy(wb_ref.at[:, pl.ds(0, PAIR * n_size)], wbs.at[s], w_sem.at[s, 1]).wait()

        def project(a):
            values = jnp.dot(xs[a], wxs[s], preferred_element_type=F32)
            for c in range(vtiles):
                pres[a % 2][c] = rounded(values[:, c * LANES:(c + 1) * LANES])
            keys = jnp.dot(xs[a], wbs[s], preferred_element_type=F32)
            for c in range(ktiles):
                pres[a % 2][vtiles + c] = rounded(keys[:, c * LANES:(c + 1) * LANES])

        def conv(a, c):
            if c < vtiles:
                at = pl.multiple_of(s * (PAIR * gcols) + c * LANES, LANES)
            else:
                at = pl.multiple_of(inner + s * (PAIR * n_size) + (c - vtiles) * LANES, LANES)
            acc = cb_ref[:, pl.ds(at, LANES)]
            w = cw_ref[:, pl.ds(at, LANES)]
            for o in range(taps):
                acc = acc + w[o:o + 1] * pres[a % 2][c, pl.ds(EDGE - taps + 1 + o, length), :]
            return silu(acc).astype(BF16)

        def contract(a):
            weights = wt[a, pl.ds(pl.multiple_of(s * (PAIR * ratio), PAIR * ratio), PAIR * ratio), :]
            for gp in range(PAIR):
                key = conv(a, vtiles + gp)
                parts = []
                for c in range(gp * tiles_group, (gp + 1) * tiles_group):
                    turned = conv(a, c).T
                    for r in range(heads_tile):
                        h = c * heads_tile + r
                        part = turned[r * p_size:(r + 1) * p_size].astype(F32)
                        parts.append((weights[h:h + 1] * part).astype(BF16))
                scaled = jnp.concatenate(parts, axis=0)
                g = s * PAIR + gp
                st_out[a, g] = jnp.dot(scaled, key, preferred_element_type=F32).astype(BF16)

        def send(a):
            for gp in range(PAIR):
                q, remote, local = state_copy(a, s * PAIR + gp)
                either(a, q, remote.start, local.start)

        for a in range(spt):
            project(a)
            if a > 0:
                contract(a - 1)
        contract(spt - 1)
        for a in range(spt):
            send(a)
        return carry

    lax.fori_loop(0, steps, step, 0)

    newest = jnp.broadcast_to(xn_ref[...].astype(F32), (EDGE, xn_ref.shape[1])).astype(BF16)
    nt[EDGE:2 * EDGE, :] = newest
    tail(0, 0)[0].wait_recv()
    for c in new_copies:
        c.wait()

    def new_conv(w_ref, start, width):
        pre = rounded(jnp.dot(nt[...], w_ref[...], preferred_element_type=F32))
        start = pl.multiple_of(start, LANES)
        acc = cb_ref[:, pl.ds(start, width)]
        w = cw_ref[:, pl.ds(start, width)]
        for o in range(taps):
            at = EDGE - taps + 1 + o
            acc = acc + w[o:o + 1] * pre[at:at + 1]
        return rounded(silu(acc))

    new_values = new_conv(wxn, vcol, hl * p_size)
    new_keys = new_conv(wbn, inner + gcol, gl * n_size)
    new_query = new_conv(wcn, inner + keys_all + gcol, gl * n_size)
    gate = rounded(jnp.dot(newest, wzn[...], preferred_element_type=F32)[0:1])
    new_raw = rounded(jnp.dot(newest, wdts[...], preferred_element_type=F32)[0:1])
    new_steps = softplus(new_raw + dtb_ref[...])
    head_s[...] = jnp.zeros_like(head_s)
    head_s[0:1, :] = new_steps
    head_s[1:2, :] = jnp.exp(-jnp.exp(alog_ref[...]) * new_steps)
    head_s[2:3, :] = dskip_ref[...]
    hrow = lax.broadcasted_iota(jnp.int32, (heads, hl * p_size), 0)
    hcol = lax.broadcasted_iota(jnp.int32, (heads, hl * p_size), 1)
    first = j * hl
    onehot = ((hcol >= (hrow - first) * p_size) & (hcol < (hrow - first + 1) * p_size)).astype(F32)
    spread_rows = jnp.dot(head_s[...], onehot, precision=lax.Precision.HIGHEST, preferred_element_type=F32)
    step_row, decay_row, skip_row = spread_rows[0:1], spread_rows[1:2], spread_rows[2:3]

    for k in range(sp):
        pltpu.make_async_remote_copy(
            src_ref=tot_out.at[0, 0], dst_ref=tot_in.at[k], send_sem=tot_send.at[0, 0],
            recv_sem=tot_recv.at[k], device_id={"sp": after, "tp": j}, device_id_type=MESH).wait_recv()
    rate_local = rate_s[j]
    factors = [None] * sp
    later_sum = jnp.zeros((hl, LANES), F32)
    for k in reversed(range(sp)):
        factors[k] = jnp.exp(rate_local * later_sum)
        later_sum = later_sum + tot_in[k]
    for g in range(gl):
        for k in range(sp):
            pltpu.make_async_remote_copy(
                src_ref=st_out.at[0, 0], dst_ref=st_in.at[k, g], send_sem=st_send.at[0, 0],
                recv_sem=st_recv.at[k, g], device_id={"sp": after, "tp": j}, device_id_type=MESH).wait_recv()
        query = new_query[:, g * n_size:(g + 1) * n_size]
        key = new_keys[:, g * n_size:(g + 1) * n_size]
        query_rows = jnp.broadcast_to(query, (EDGE, n_size)).astype(BF16)
        helds = []
        for r in range(ratio):
            h = g * ratio + r
            acc = jnp.zeros((p_size, n_size), F32)
            for k in range(sp):
                acc += factors[k][h:h + 1] * st_in[k, g, r * p_size:(r + 1) * p_size, :].astype(F32)
            top = acc.astype(BF16)
            state_ref[0, h] = top
            held = jnp.zeros((EDGE, p_size), F32)
            rest = acc
            for _ in range(3):
                term = rest.astype(BF16)
                held += lax.dot_general(query_rows, term, (((1,), (1,)), ((), ())), preferred_element_type=F32)
                rest = rest - term.astype(F32)
            helds.append(held[0:1])
        span = slice(g * gcols, (g + 1) * gcols)
        held_row = jnp.concatenate(helds, axis=1)
        inner_prod = jnp.sum(query * key, axis=1, keepdims=True)
        value_row = new_values[:, span]
        out = (decay_row[:, span] * held_row + (step_row[:, span] * inner_prod) * value_row
               + skip_row[:, span] * value_row)
        gated = out * silu(gate[:, span])
        ms = jnp.sum(gated * gated, axis=1, keepdims=True) / gcols
        normed = gated * lax.rsqrt(ms + EPS)
        for r in range(ratio):
            h = g * ratio + r
            read_s[h:h + 1, :] = normed[:, r * p_size:(r + 1) * p_size] * ng_ref[h:h + 1, :]
    read_ref[0] = read_s[...].astype(BF16)

    @pl.when(i == sp - 1)
    def _():
        for a in range(spt):
            for q in range(tp):
                either(a, q, tail(a, q)[0].wait_send, None)
    for a in range(spt):
        for q in range(tp):
            either(a, q, tot(a, q)[0].wait_send, None)
        for g in range(groups):
            q, remote, _ = state_copy(a, g)
            either(a, q, remote.wait_send, None)


def per_device(
    dims, x_in, x_new, w_x, w_b, w_c, w_dt, w_z, conv_w, conv_b, dt_bias, a_log, d_skip, norm_g
):
    sp, tp, heads, groups, n_size, p_size, ratio, taps = dims
    spt, length, width = x_in.shape
    hl, gl = heads // tp, groups // tp
    assert x_new.shape[0] == 1 and sp == spt * tp and spt <= 2
    steps, gcols = groups // PAIR, ratio * p_size
    tiles = PAIR * (gcols + n_size) // LANES
    any_spec = pl.BlockSpec(memory_space=pl.ANY)
    vmem = pl.BlockSpec(memory_space=pltpu.VMEM)
    dma = pltpu.SemaphoreType.DMA
    return pl.pallas_call(
        functools.partial(kernel, dims),
        out_shape=(
            jax.ShapeDtypeStruct((1, hl, p_size, n_size), BF16),
            jax.ShapeDtypeStruct((1, hl, p_size), BF16),
        ),
        in_specs=[any_spec, vmem] + [any_spec] * 5 + [vmem] * 6,
        out_specs=(vmem, vmem),
        scratch_shapes=[
            pltpu.VMEM((spt, EDGE + length, width), BF16),
            pltpu.VMEM((steps, width, PAIR * gcols), BF16),
            pltpu.VMEM((steps, width, PAIR * n_size), BF16),
            pltpu.VMEM((width, heads), BF16),
            pltpu.VMEM((width, hl * p_size), BF16),
            pltpu.VMEM((width, gl * n_size), BF16),
            pltpu.VMEM((width, gl * n_size), BF16),
            pltpu.VMEM((width, hl * p_size), BF16),
            pltpu.VMEM((2 * EDGE, width), BF16),
            pltpu.VMEM((tiles, EDGE + length, LANES), F32),
            pltpu.VMEM((tiles, EDGE + length, LANES), F32),
            pltpu.VMEM((length, LANES), F32),
            pltpu.VMEM((spt, heads, length), F32),
            pltpu.VMEM((spt, tp, hl, LANES), F32),
            pltpu.VMEM((sp, hl, LANES), F32),
            pltpu.VMEM((tp, hl, LANES), F32),
            pltpu.VMEM((spt, groups, gcols, n_size), BF16),
            pltpu.VMEM((sp, gl, gcols, n_size), BF16),
            pltpu.VMEM((8, heads), F32),
            pltpu.VMEM((hl, p_size), F32),
            dma((spt,)), dma, dma((steps, 2)), dma((4,)), dma((spt,)), dma((spt,)),
            dma((spt, tp)), dma((1,)), dma((spt, tp)), dma((sp,)), dma((spt, groups)), dma((sp, gl)),
        ],
        compiler_params=pltpu.CompilerParams(
            collective_id=0, has_side_effects=True, vmem_limit_bytes=60 * 1024 * 1024
        ),
    )(
        x_in, x_new, w_x, w_b, w_c, w_dt, w_z, conv_w, conv_b.reshape(1, -1),
        dt_bias.reshape(1, -1), a_log.reshape(1, -1), d_skip.reshape(1, -1), norm_g,
    )


def solution(mesh):
    sp, tp = mesh.shape["sp"], mesh.shape["tp"]

    def step(x_in, x_new, w_x, w_b, w_c, w_dt, w_z, conv_w, conv_b, dt_bias, a_log, d_skip, norm_g):
        heads, p_size = w_dt.shape[1], norm_g.shape[1]
        keys_all = w_b.shape[1]
        n_size = LANES
        groups = keys_all // n_size
        dims = (sp, tp, heads, groups, n_size, p_size, heads // groups, conv_w.shape[0])
        return per_device(
            dims, x_in, x_new, w_x, w_b, w_c, w_dt, w_z, conv_w, conv_b, dt_bias, a_log, d_skip, norm_g)

    return jax.shard_map(
        step,
        mesh=mesh,
        in_specs=(
            P("tp", "sp", None), P("sp", None), P(), P(), P(), P(), P(None, "tp"),
            P(), P(), P(), P(), P(), P("tp", None),
        ),
        out_specs=(P("sp", "tp", None, None), P("sp", "tp", None)),
        check_vma=False,
    )
```

time: 259 us -> 74.7 us (0.29)
  the two profiles are of different devices: /device:TPU:5 before, /device:TPU:7 now
where the time goes in v1:
time: 74.7 us; the launch traced here: 74.4 us
  Pallas kernels  69.1 us (93%)
  local copies, waits for them, and re-layouts  4.71 us (6%)
    pallas_call x1, Pallas kernels, per_device(): pl.pallas_call(functools.partial(kernel, dims), out_shape=(jax.ShapeDtype...  69.1 us
    unnamed x3, local copies, waits for them, and re-layouts  4.71 us

profile of v1, /device:TPU:7, one launch (start us, length us, event | category | flops | bytes accessed | tf_op | source)
XLA Modules:
  0.0 74.4 jit_solution(17485586866884345873)
XLA Ops:
  0.6 1.9 %copy.15.wdt_ref = bf16[2048,32]{1,0:T(8,128)(2,1)} copy(bf16[2048,32]{0,1:T(8,128)(2,1)} %param.18) | data formatting | bytes 262144 | tf_op args[5]
  2.5 69.1 %shard_map.140 = (bf16[1,8,64,128]{3,2,1,0:T(8,128)(2,1)}, bf16[1,8,64]{2,1,0:T(8,128)(2,1)}) custom-call(bf16[2,384,2048]{2,1,0:T(8,128)(2,1)} %x_ref.1, bf16[1,2048]{1,0:T(2,128)(2,1)} %xn_ref.1, bf16[2048,2048]{1,0:T(8,128)(2,1)} %wx_ref.1, bf16[2048,1024]{1,0:T(8,128)(2,1)} %wb_ref.1, bf16[2048,1024]{1,0:T(8,128)(2,1)} %wc_ref.1, ...), custom_call_target="tpu_custom_call" | custom-call | tf_op jit(solution)/shard_map/pallas_call | solution.py:342
  71.6 1.6 %copy.18 = bf16[1,8,64,128]{3,2,1,0:T(8,128)(2,1)} copy(bf16[1,8,64,128]{3,2,1,0:T(8,128)(2,1)} %get-tuple-element.4) | data formatting | bytes 262144
  73.2 1.2 %copy.19 = bf16[1,8,64]{2,1,0:T(8,128)(2,1)} copy(bf16[1,8,64]{2,1,0:T(8,128)(2,1)} %get-tuple-element.5) | data formatting | bytes 2048

commit v2 on v1

--- a/solution.py
+++ b/solution.py
@@ -32,12 +32,12 @@
 def kernel(
     dims,
     x_ref, xn_ref, wx_ref, wb_ref, wc_ref, wdt_ref, wz_ref,
-    cw_ref, cb_ref, dtb_ref, alog_ref, dskip_ref, ng_ref,
+    cw_hbm, cb_hbm, dtb_ref, alog_ref, dskip_ref, ng_ref,
     state_ref, read_ref,
     xs, wxs, wbs, wdts, wxn, wbn, wcn, wzn, nt, pre0, pre1, padded,
-    wt, tot_out, tot_in, rate_s, st_out, st_in, head_s, read_s,
-    x_sem, wdt_sem, w_sem, new_sem, halo_send, halo_recv, tail_send, tail_recv,
-    tot_send, tot_recv, st_send, st_recv,
+    wt, tot_out, tot_in, a_out, a_in, mine, b_in, st_out, st_in, head_s, read_s, cw_ref, cb_ref,
+    x_sem, wdt_sem, w_sem, new_sem, conv_sem, halo_send, halo_recv, tail_send, tail_recv,
+    tot_send, tot_recv, a_send, a_recv, b_send, b_recv, st_send, st_recv,
 ):
     sp, tp, heads, groups, n_size, p_size, ratio, taps = dims
     i, j = lax.axis_index("sp"), lax.axis_index("tp")
@@ -47,16 +47,24 @@
     gcols = ratio * p_size
     steps = groups // PAIR
     home = i // spt
-    own = home == j
     pres = (pre0, pre1)
+    member, m = lax.rem(i, 2), i // 2
+    direct = m // 2 == j // 2
+    near = jnp.logical_not(direct) & ((j > m) == (lax.rem(m, 2) == 1))
+    far = jnp.logical_not(direct) & jnp.logical_not(near)
+    partner, sibling = i + 1 - 2 * member, i + 2 - 4 * lax.rem(m, 2)
+    pairs = sp // 4
 
     barrier = pltpu.get_barrier_semaphore()
     for k in range(sp):
-        @pl.when(jnp.logical_not(own & (i == k)))
+        @pl.when(i != k)
+        def _():
+            pl.semaphore_signal(barrier, inc=1, device_id={"sp": k, "tp": j}, device_id_type=MESH)
+
+        @pl.when(home != j)
         def _():
             pl.semaphore_signal(barrier, inc=1, device_id={"sp": k, "tp": home}, device_id_type=MESH)
-    before, after = lax.rem(i + sp - 1, sp), lax.rem(i + 1, sp)
-    pl.semaphore_signal(barrier, inc=1, device_id={"sp": before, "tp": j}, device_id_type=MESH)
+    after = lax.rem(i + 1, sp)
 
     wdt_copy = pltpu.make_async_copy(wdt_ref, wdts, wdt_sem)
     x_copies = [
@@ -79,16 +87,25 @@
         pltpu.make_async_copy(wc_ref.at[:, pl.ds(gcol, gl * n_size)], wcn, new_sem.at[2]),
         pltpu.make_async_copy(wz_ref, wzn, new_sem.at[3]),
     ]
+    conv_copies = [
+        pltpu.make_async_copy(cw_hbm, cw_ref, conv_sem.at[0]),
+        pltpu.make_async_copy(cb_hbm, cb_ref, conv_sem.at[1]),
+    ]
     wdt_copy.start()
     for c in x_copies:
         c.start()
-    for pair in w_copies:
+    for pair in w_copies[:1]:
+        for c in pair:
+            c.start()
+    for c in conv_copies:
+        c.start()
+    for pair in w_copies[1:]:
         for c in pair:
             c.start()
     for c in new_copies:
         c.start()
 
-    pl.semaphore_wait(barrier, spt * tp + 1 - own.astype(jnp.int32))
+    pl.semaphore_wait(barrier, sp - 1 + spt * (tp - 1))
 
     def halo(a):
         return pltpu.make_async_remote_copy(
@@ -124,29 +141,31 @@
                 either(a, q, remote.start, local.start)
 
     padded[...] = jnp.zeros_like(padded)
-    padded[0:1, 0:heads] = alog_ref[...]
-    spread = jnp.broadcast_to(padded[0:1, :], (LANES, LANES)).T[0:heads]
-    rates = -jnp.exp(spread)
-    for q in range(tp):
-        rate_s[q] = rates[q * hl:(q + 1) * hl]
-    padded[0:1, 0:heads] = jnp.zeros((1, heads), F32)
+
+    def column(row):
+        padded[0:1, 0:heads] = row
+        return jnp.broadcast_to(padded[0:1, :], (LANES, LANES)).T[0:heads]
+
+    rate_row = -jnp.exp(alog_ref[...])
+    rates = column(rate_row)
 
     rows = lax.broadcasted_iota(jnp.int32, (length, length), 0)
     cols = lax.broadcasted_iota(jnp.int32, (length, length), 1)
     later = (rows > cols).astype(F32).astype(BF16)
     wdt_copy.wait()
 
-    def tot(a, q):
-        src, dst = tot_out.at[a, q], tot_in.at[i]
+    def tot(k):
         return pltpu.make_async_remote_copy(
-            src_ref=src, dst_ref=dst, send_sem=tot_send.at[a, q], recv_sem=tot_recv.at[i],
-            device_id={"sp": spt * j + a, "tp": q}, device_id_type=MESH
-        ), pltpu.make_async_copy(src, dst, tot_recv.at[i])
-
+            src_ref=tot_out, dst_ref=tot_in.at[i], send_sem=tot_send.at[k], recv_sem=tot_recv.at[i],
+            device_id={"sp": k, "tp": j}, device_id_type=MESH)
+
+    tot_out[...] = jnp.zeros_like(tot_out)
     for a in range(spt):
         x_copies[a].wait()
-        raw = jnp.dot(xs[a, EDGE:, :], wdts[...], preferred_element_type=F32)
+        raw = lax.dot_general(
+            xs[a, EDGE:, :], wdts[...], (((1,), (1,)), ((), ())), preferred_element_type=F32)
         padded[:, 0:heads] = softplus(rounded(raw) + dtb_ref[...])
+        tot_out[a:a + 1, :] = jnp.sum(padded[...], axis=0, keepdims=True)
         sizes = padded[...].T[0:heads]
         rest = jnp.zeros_like(sizes)
         left = sizes
@@ -155,26 +174,82 @@
             rest += jnp.dot(term, later, preferred_element_type=F32)
             left = left - term.astype(F32)
         wt[a] = jnp.exp(rates[:, 0:1] * rest) * sizes
-        total = jnp.broadcast_to(rest[:, 0:1] + sizes[:, 0:1], (heads, LANES))
-        for q in range(tp):
-            tot_out[a, q] = total[q * hl:(q + 1) * hl]
-    for a in range(spt):
-        for q in range(tp):
-            remote, local = tot(a, q)
-            either(a, q, remote.start, local.start)
+    tot_in[i] = tot_out[...]
+    for k in range(sp):
+        pl.when(i != k)(tot(k).start)
 
     for a in range(spt):
         halo(a).wait()
         xs[a, 0:EDGE, :] = jnp.where(i == 0, 0.0, xs[a, 0:EDGE, :].astype(F32)).astype(BF16)
 
-    def state_copy(a, g):
+    for k in range(sp):
+        @pl.when(i != k)
+        def _():
+            pltpu.make_async_remote_copy(
+                src_ref=tot_out, dst_ref=tot_in.at[k], send_sem=tot_send.at[k], recv_sem=tot_recv.at[k],
+                device_id={"sp": k, "tp": j}, device_id_type=MESH).wait_recv()
+    beyond = jnp.zeros(tot_out.shape, F32)
+    for k in range(sp):
+        beyond = beyond + jnp.where(k > i, tot_in[k], 0.0)
+    for a in range(spt):
+        wt[a] = wt[a] * column(jnp.exp(rate_row * beyond[a:a + 1, 0:heads]))[:, 0:1]
+
+    def a_copy(s):
+        return pltpu.make_async_remote_copy(
+            src_ref=a_out.at[s], dst_ref=a_in.at[s], send_sem=a_send.at[s], recv_sem=a_recv.at[s],
+            device_id={"sp": partner, "tp": j}, device_id_type=MESH)
+
+    def b_copy(s):
+        return pltpu.make_async_remote_copy(
+            src_ref=st_out.at[s], dst_ref=b_in.at[s], send_sem=b_send.at[s], recv_sem=b_recv.at[s],
+            device_id={"sp": sibling, "tp": j}, device_id_type=MESH)
+
+    slot = jnp.where(direct & (lax.rem(m, 2) == 1), pairs, m // 2)
+
+    def state_copy(s, gp):
+        g = s * PAIR + gp
         q = g // gl
-        src, dst = st_out.at[a, g], st_in.at[i, lax.rem(g, gl)]
-        sem = st_recv.at[i, lax.rem(g, gl)]
-        return q, pltpu.make_async_remote_copy(
-            src_ref=src, dst_ref=dst, send_sem=st_send.at[a, g], recv_sem=sem,
-            device_id={"sp": spt * j + a, "tp": q}, device_id_type=MESH
+        src, dst = st_out.at[s, gp], st_in.at[slot, lax.rem(g, gl)]
+        sem = st_recv.at[slot, lax.rem(g, gl)]
+        return (m == j) & (q == j), pltpu.make_async_remote_copy(
+            src_ref=src, dst_ref=dst, send_sem=st_send.at[s, gp], recv_sem=sem,
+            device_id={"sp": spt * j + member, "tp": q}, device_id_type=MESH
         ), pltpu.make_async_copy(src, dst, sem)
+
+    def pass_on(s):
+        a_copy(s).wait_recv()
+
+        def add(*more):
+            for gp in range(PAIR):
+                for r in range(0, gcols, LANES):
+                    total = mine[s, gp, r:r + LANES, :].astype(F32)
+                    for ref in more:
+                        total += ref[s, gp, r:r + LANES, :].astype(F32)
+                    st_out[s, gp, r:r + LANES, :] = total.astype(BF16)
+
+        @pl.when(near)
+        def _():
+            b_copy(s).wait_recv()
+            add(a_in, b_in)
+
+        @pl.when(jnp.logical_not(near))
+        def _():
+            add(a_in)
+
+        @pl.when(far)
+        def _():
+            b_copy(s).start()
+
+        @pl.when(jnp.logical_not(far))
+        def _():
+            for gp in range(PAIR):
+                here, remote, local = state_copy(s, gp)
+                pl.when(jnp.logical_not(here))(remote.start)
+                pl.when(here)(local.start)
+
+    lag = jnp.where(near, 2, 1)
+    for c in conv_copies:
+        c.wait()
 
     vtiles, ktiles = PAIR * gcols // LANES, PAIR * n_size // LANES
     tiles_group = gcols // LANES
@@ -215,24 +290,26 @@
                         part = turned[r * p_size:(r + 1) * p_size].astype(F32)
                         parts.append((weights[h:h + 1] * part).astype(BF16))
                 scaled = jnp.concatenate(parts, axis=0)
-                g = s * PAIR + gp
-                st_out[a, g] = jnp.dot(scaled, key, preferred_element_type=F32).astype(BF16)
-
-        def send(a):
-            for gp in range(PAIR):
-                q, remote, local = state_copy(a, s * PAIR + gp)
-                either(a, q, remote.start, local.start)
-
+                term = jnp.dot(scaled, key, preferred_element_type=F32)
+                terms[a].append(term.astype(BF16))
+
+        terms = [[] for _ in range(spt)]
         for a in range(spt):
             project(a)
             if a > 0:
                 contract(a - 1)
         contract(spt - 1)
-        for a in range(spt):
-            send(a)
+        for gp in range(PAIR):
+            first, second = (terms[a][gp].astype(F32) for a in range(2))
+            a_out[s, gp] = jnp.where(member == 0, second, first).astype(BF16)
+            mine[s, gp] = jnp.where(member == 0, first, second).astype(BF16)
+        a_copy(s).start()
+        pl.when(s >= lag)(lambda: pass_on(s - lag))
         return carry
 
     lax.fori_loop(0, steps, step, 0)
+    pass_on(steps - lag)
+    pl.when(near)(lambda: pass_on(steps - 1))
 
     newest = jnp.broadcast_to(xn_ref[...].astype(F32), (EDGE, xn_ref.shape[1])).astype(BF16)
     nt[EDGE:2 * EDGE, :] = newest
@@ -254,7 +331,8 @@
     new_keys = new_conv(wbn, inner + gcol, gl * n_size)
     new_query = new_conv(wcn, inner + keys_all + gcol, gl * n_size)
     gate = rounded(jnp.dot(newest, wzn[...], preferred_element_type=F32)[0:1])
-    new_raw = rounded(jnp.dot(newest, wdts[...], preferred_element_type=F32)[0:1])
+    new_raw = rounded(lax.dot_general(
+        newest, wdts[...], (((1,), (1,)), ((), ())), preferred_element_type=F32)[0:1])
     new_steps = softplus(new_raw + dtb_ref[...])
     head_s[...] = jnp.zeros_like(head_s)
     head_s[0:1, :] = new_steps
@@ -267,18 +345,8 @@
     spread_rows = jnp.dot(head_s[...], onehot, precision=lax.Precision.HIGHEST, preferred_element_type=F32)
     step_row, decay_row, skip_row = spread_rows[0:1], spread_rows[1:2], spread_rows[2:3]
 
-    for k in range(sp):
-        pltpu.make_async_remote_copy(
-            src_ref=tot_out.at[0, 0], dst_ref=tot_in.at[k], send_sem=tot_send.at[0, 0],
-            recv_sem=tot_recv.at[k], device_id={"sp": after, "tp": j}, device_id_type=MESH).wait_recv()
-    rate_local = rate_s[j]
-    factors = [None] * sp
-    later_sum = jnp.zeros((hl, LANES), F32)
-    for k in reversed(range(sp)):
-        factors[k] = jnp.exp(rate_local * later_sum)
-        later_sum = later_sum + tot_in[k]
     for g in range(gl):
-        for k in range(sp):
+        for k in range(pairs + 1):
             pltpu.make_async_remote_copy(
                 src_ref=st_out.at[0, 0], dst_ref=st_in.at[k, g], send_sem=st_send.at[0, 0],
                 recv_sem=st_recv.at[k, g], device_id={"sp": after, "tp": j}, device_id_type=MESH).wait_recv()
@@ -289,8 +357,8 @@
         for r in range(ratio):
             h = g * ratio + r
             acc = jnp.zeros((p_size, n_size), F32)
-            for k in range(sp):
-                acc += factors[k][h:h + 1] * st_in[k, g, r * p_size:(r + 1) * p_size, :].astype(F32)
+            for k in range(pairs + 1):
+                acc += st_in[k, g, r * p_size:(r + 1) * p_size, :].astype(F32)
             top = acc.astype(BF16)
             state_ref[0, h] = top
             held = jnp.zeros((EDGE, p_size), F32)
@@ -319,12 +387,14 @@
         for a in range(spt):
             for q in range(tp):
                 either(a, q, tail(a, q)[0].wait_send, None)
-    for a in range(spt):
-        for q in range(tp):
-            either(a, q, tot(a, q)[0].wait_send, None)
-        for g in range(groups):
-            q, remote, _ = state_copy(a, g)
-            either(a, q, remote.wait_send, None)
+    for k in range(sp):
+        pl.when(i != k)(tot(k).wait_send)
+    for s in range(steps):
+        a_copy(s).wait_send()
+        pl.when(far)(b_copy(s).wait_send)
+        for gp in range(PAIR):
+            here, remote, _ = state_copy(s, gp)
+            pl.when(jnp.logical_not(far) & jnp.logical_not(here))(remote.wait_send)
 
 
 def per_device(
@@ -333,7 +403,7 @@
     sp, tp, heads, groups, n_size, p_size, ratio, taps = dims
     spt, length, width = x_in.shape
     hl, gl = heads // tp, groups // tp
-    assert x_new.shape[0] == 1 and sp == spt * tp and spt <= 2
+    assert x_new.shape[0] == 1 and sp == spt * tp and spt == 2 and sp % 4 == 0
     steps, gcols = groups // PAIR, ratio * p_size
     tiles = PAIR * (gcols + n_size) // LANES
     any_spec = pl.BlockSpec(memory_space=pl.ANY)
@@ -345,13 +415,13 @@
             jax.ShapeDtypeStruct((1, hl, p_size, n_size), BF16),
             jax.ShapeDtypeStruct((1, hl, p_size), BF16),
         ),
-        in_specs=[any_spec, vmem] + [any_spec] * 5 + [vmem] * 6,
+        in_specs=[any_spec, vmem] + [any_spec] * 7 + [vmem] * 4,
         out_specs=(vmem, vmem),
         scratch_shapes=[
             pltpu.VMEM((spt, EDGE + length, width), BF16),
             pltpu.VMEM((steps, width, PAIR * gcols), BF16),
             pltpu.VMEM((steps, width, PAIR * n_size), BF16),
-            pltpu.VMEM((width, heads), BF16),
+            pltpu.VMEM((heads, width), BF16),
             pltpu.VMEM((width, hl * p_size), BF16),
             pltpu.VMEM((width, gl * n_size), BF16),
             pltpu.VMEM((width, gl * n_size), BF16),
@@ -361,21 +431,27 @@
             pltpu.VMEM((tiles, EDGE + length, LANES), F32),
             pltpu.VMEM((length, LANES), F32),
             pltpu.VMEM((spt, heads, length), F32),
-            pltpu.VMEM((spt, tp, hl, LANES), F32),
-            pltpu.VMEM((sp, hl, LANES), F32),
-            pltpu.VMEM((tp, hl, LANES), F32),
-            pltpu.VMEM((spt, groups, gcols, n_size), BF16),
-            pltpu.VMEM((sp, gl, gcols, n_size), BF16),
+            pltpu.VMEM((8, LANES), F32),
+            pltpu.VMEM((sp, 8, LANES), F32),
+            pltpu.VMEM((steps, PAIR, gcols, n_size), BF16),
+            pltpu.VMEM((steps, PAIR, gcols, n_size), BF16),
+            pltpu.VMEM((steps, PAIR, gcols, n_size), BF16),
+            pltpu.VMEM((steps, PAIR, gcols, n_size), BF16),
+            pltpu.VMEM((steps, PAIR, gcols, n_size), BF16),
+            pltpu.VMEM((sp // 4 + 1, gl, gcols, n_size), BF16),
             pltpu.VMEM((8, heads), F32),
             pltpu.VMEM((hl, p_size), F32),
-            dma((spt,)), dma, dma((steps, 2)), dma((4,)), dma((spt,)), dma((spt,)),
-            dma((spt, tp)), dma((1,)), dma((spt, tp)), dma((sp,)), dma((spt, groups)), dma((sp, gl)),
+            pltpu.VMEM(conv_w.shape, F32),
+            pltpu.VMEM((1, conv_w.shape[1]), F32),
+            dma((spt,)), dma, dma((steps, 2)), dma((4,)), dma((2,)), dma((spt,)), dma((spt,)),
+            dma((spt, tp)), dma((1,)), dma((sp,)), dma((sp,)), dma((steps,)), dma((steps,)),
+            dma((steps,)), dma((steps,)), dma((steps, PAIR)), dma((sp // 4 + 1, gl)),
         ],
         compiler_params=pltpu.CompilerParams(
             collective_id=0, has_side_effects=True, vmem_limit_bytes=60 * 1024 * 1024
         ),
     )(
-        x_in, x_new, w_x, w_b, w_c, w_dt, w_z, conv_w, conv_b.reshape(1, -1),
+        x_in, x_new, w_x, w_b, w_c, w_dt.T, w_z, conv_w, conv_b.reshape(1, -1),
         dt_bias.reshape(1, -1), a_log.reshape(1, -1), d_skip.reshape(1, -1), norm_g,
     )
 

time: 74.7 us -> 54.2 us (0.73)
  the two profiles are of different devices: /device:TPU:7 before, /device:TPU:5 now
where the time goes in v2:
time: 54.2 us; the launch traced here: 53.9 us
  Pallas kernels  50.4 us (93%)
  local copies, waits for them, and re-layouts  2.83 us (5%)
  between operations  0.64 us (1%)
    pallas_call x1, Pallas kernels, per_device(): pl.pallas_call(functools.partial(kernel, dims), out_shape=(jax.ShapeDtype...  50.4 us
    unnamed x2, local copies, waits for them, and re-layouts  2.83 us

profile of v2, /device:TPU:5, one launch (start us, length us, event | category | flops | bytes accessed | tf_op | source)
XLA Modules:
  0.0 53.9 jit_solution(10959003328003839959)
XLA Ops:
  0.6 50.4 %shard_map.140 = (bf16[1,8,64,128]{3,2,1,0:T(8,128)(2,1)}, bf16[1,8,64]{2,1,0:T(8,128)(2,1)}) custom-call(bf16[2,384,2048]{2,1,0:T(8,128)(2,1)} %x_ref.1, bf16[1,2048]{1,0:T(2,128)(2,1)} %xn_ref.1, bf16[2048,2048]{1,0:T(8,128)(2,1)} %wx_ref.1, bf16[2048,1024]{1,0:T(8,128)(2,1)} %wb_ref.1, bf16[2048,1024]{1,0:T(8,128)(2,1)} %wc_ref.1, ...), custom_call_target="tpu_custom_call" | custom-call | tf_op jit(solution)/shard_map/pallas_call | solution.py:412
  51.1 1.6 %copy.17 = bf16[1,8,64,128]{3,2,1,0:T(8,128)(2,1)} copy(bf16[1,8,64,128]{3,2,1,0:T(8,128)(2,1)} %get-tuple-element.4) | data formatting | bytes 262144
  52.7 1.3 %copy.18 = bf16[1,8,64]{2,1,0:T(8,128)(2,1)} copy(bf16[1,8,64]{2,1,0:T(8,128)(2,1)} %get-tuple-element.5) | data formatting | bytes 2048

commit v3 on v2

--- a/solution.py
+++ b/solution.py
@@ -12,6 +12,7 @@
 BF16 = jnp.bfloat16
 EPS = 1e-05
 EDGE = 16
+SENT = 8
 PAIR = 2
 LANES = 128
 
@@ -35,8 +36,8 @@
     cw_hbm, cb_hbm, dtb_ref, alog_ref, dskip_ref, ng_ref,
     state_ref, read_ref,
     xs, wxs, wbs, wdts, wxn, wbn, wcn, wzn, nt, pre0, pre1, padded,
-    wt, tot_out, tot_in, a_out, a_in, mine, b_in, st_out, st_in, head_s, read_s, cw_ref, cb_ref,
-    x_sem, wdt_sem, w_sem, new_sem, conv_sem, halo_send, halo_recv, tail_send, tail_recv,
+    wt, tot_out, tot_in, fcol, terms, a_out, a_in, mine, b_in, st_out, st_in, head_s, read_s, cw_ref, cb_ref,
+    x_sem, wdt_sem, w_sem, new_sem, conv_sem, halo_send, halo_recv, tail_send, tail_recv, relay_send,
     tot_send, tot_recv, a_send, a_recv, b_send, b_recv, st_send, st_recv,
 ):
     sp, tp, heads, groups, n_size, p_size, ratio, taps = dims
@@ -54,6 +55,10 @@
     far = jnp.logical_not(direct) & jnp.logical_not(near)
     partner, sibling = i + 1 - 2 * member, i + 2 - 4 * lax.rem(m, 2)
     pairs = sp // 4
+
+    nt[0:EDGE - SENT, :] = jnp.zeros((EDGE - SENT, nt.shape[1]), BF16)
+    for a in range(spt):
+        xs[a, 0:EDGE - SENT, :] = jnp.zeros((EDGE - SENT, nt.shape[1]), BF16)
 
     barrier = pltpu.get_barrier_semaphore()
     for k in range(sp):
@@ -109,36 +114,35 @@
 
     def halo(a):
         return pltpu.make_async_remote_copy(
-            src_ref=x_ref.at[a, pl.ds(length - EDGE, EDGE)],
-            dst_ref=xs.at[a, pl.ds(0, EDGE)],
+            src_ref=x_ref.at[a, pl.ds(length - SENT, SENT)],
+            dst_ref=xs.at[a, pl.ds(EDGE - SENT, SENT)],
             send_sem=halo_send.at[a], recv_sem=halo_recv.at[a],
             device_id={"sp": after, "tp": j}, device_id_type=MESH)
 
     for a in range(spt):
         halo(a).start()
 
-    def is_self(a, q):
-        return (spt * j + a == i) & (j == q)
-
-    def either(a, q, remote, local):
-        here = is_self(a, q)
-        pl.when(jnp.logical_not(here))(remote)
-        if local is not None:
-            pl.when(here)(local)
-
-    def tail(a, q):
-        src, dst = x_ref.at[a, pl.ds(length - EDGE, EDGE)], nt.at[pl.ds(0, EDGE)]
+    root = home == j
+
+    def tail(a):
+        src, dst = x_ref.at[a, pl.ds(length - SENT, SENT)], nt.at[pl.ds(EDGE - SENT, SENT)]
+        return spt * j + a == i, pltpu.make_async_remote_copy(
+            src_ref=src, dst_ref=dst, send_sem=tail_send.at[a], recv_sem=tail_recv.at[0],
+            device_id={"sp": spt * j + a, "tp": j}, device_id_type=MESH
+        ), pltpu.make_async_copy(src, dst, tail_recv.at[0])
+
+    def relay(q):
+        rows = nt.at[pl.ds(EDGE - SENT, SENT)]
         return pltpu.make_async_remote_copy(
-            src_ref=src, dst_ref=dst, send_sem=tail_send.at[a, q], recv_sem=tail_recv.at[0],
-            device_id={"sp": spt * j + a, "tp": q}, device_id_type=MESH
-        ), pltpu.make_async_copy(src, dst, tail_recv.at[0])
+            src_ref=rows, dst_ref=rows, send_sem=relay_send.at[q], recv_sem=tail_recv.at[0],
+            device_id={"sp": i, "tp": q}, device_id_type=MESH)
 
     @pl.when(i == sp - 1)
     def _():
         for a in range(spt):
-            for q in range(tp):
-                remote, local = tail(a, q)
-                either(a, q, remote.start, local.start)
+            here, remote, local = tail(a)
+            pl.when(jnp.logical_not(here))(remote.start)
+            pl.when(here)(local.start)
 
     padded[...] = jnp.zeros_like(padded)
 
@@ -182,17 +186,18 @@
         halo(a).wait()
         xs[a, 0:EDGE, :] = jnp.where(i == 0, 0.0, xs[a, 0:EDGE, :].astype(F32)).astype(BF16)
 
-    for k in range(sp):
-        @pl.when(i != k)
-        def _():
-            pltpu.make_async_remote_copy(
-                src_ref=tot_out, dst_ref=tot_in.at[k], send_sem=tot_send.at[k], recv_sem=tot_recv.at[k],
-                device_id={"sp": k, "tp": j}, device_id_type=MESH).wait_recv()
-    beyond = jnp.zeros(tot_out.shape, F32)
-    for k in range(sp):
-        beyond = beyond + jnp.where(k > i, tot_in[k], 0.0)
-    for a in range(spt):
-        wt[a] = wt[a] * column(jnp.exp(rate_row * beyond[a:a + 1, 0:heads]))[:, 0:1]
+    def later_factors():
+        for k in range(sp):
+            @pl.when(i != k)
+            def _():
+                pltpu.make_async_remote_copy(
+                    src_ref=tot_out, dst_ref=tot_in.at[k], send_sem=tot_send.at[k], recv_sem=tot_recv.at[k],
+                    device_id={"sp": k, "tp": j}, device_id_type=MESH).wait_recv()
+        beyond = jnp.zeros(tot_out.shape, F32)
+        for k in range(sp):
+            beyond = beyond + jnp.where(k > i, tot_in[k], 0.0)
+        for a in range(spt):
+            fcol[a] = column(jnp.exp(rate_row * beyond[a:a + 1, 0:heads]))
 
     def a_copy(s):
         return pltpu.make_async_remote_copy(
@@ -290,30 +295,38 @@
                         part = turned[r * p_size:(r + 1) * p_size].astype(F32)
                         parts.append((weights[h:h + 1] * part).astype(BF16))
                 scaled = jnp.concatenate(parts, axis=0)
-                term = jnp.dot(scaled, key, preferred_element_type=F32)
-                terms[a].append(term.astype(BF16))
-
-        terms = [[] for _ in range(spt)]
+                terms[a, gp] = jnp.dot(scaled, key, preferred_element_type=F32)
+
         for a in range(spt):
             project(a)
             if a > 0:
                 contract(a - 1)
         contract(spt - 1)
+        pl.when(s == 0)(later_factors)
+        at = pl.multiple_of(s * (PAIR * ratio), PAIR * ratio)
+        factors = [fcol[a, pl.ds(at, PAIR * ratio), :] for a in range(spt)]
         for gp in range(PAIR):
-            first, second = (terms[a][gp].astype(F32) for a in range(2))
-            a_out[s, gp] = jnp.where(member == 0, second, first).astype(BF16)
-            mine[s, gp] = jnp.where(member == 0, first, second).astype(BF16)
+            for r in range(ratio):
+                h, span = gp * ratio + r, slice(r * p_size, (r + 1) * p_size)
+                first, second = (factors[a][h:h + 1] * terms[a, gp, span, :] for a in range(spt))
+                a_out[s, gp, span, :] = jnp.where(member == 0, second, first).astype(BF16)
+                mine[s, gp, span, :] = jnp.where(member == 0, first, second).astype(BF16)
         a_copy(s).start()
         pl.when(s >= lag)(lambda: pass_on(s - lag))
+
+        @pl.when(root & (s == steps - 1))
+        def _():
+            tail(0)[1].wait_recv()
+            for q in range(tp):
+                pl.when(q != j)(relay(q).start)
+
         return carry
 
     lax.fori_loop(0, steps, step, 0)
-    pass_on(steps - lag)
-    pl.when(near)(lambda: pass_on(steps - 1))
 
     newest = jnp.broadcast_to(xn_ref[...].astype(F32), (EDGE, xn_ref.shape[1])).astype(BF16)
     nt[EDGE:2 * EDGE, :] = newest
-    tail(0, 0)[0].wait_recv()
+    pl.when(jnp.logical_not(root))(tail(0)[1].wait_recv)
     for c in new_copies:
         c.wait()
 
@@ -345,6 +358,8 @@
     spread_rows = jnp.dot(head_s[...], onehot, precision=lax.Precision.HIGHEST, preferred_element_type=F32)
     step_row, decay_row, skip_row = spread_rows[0:1], spread_rows[1:2], spread_rows[2:3]
 
+    pass_on(steps - lag)
+    pl.when(near)(lambda: pass_on(steps - 1))
     for g in range(gl):
         for k in range(pairs + 1):
             pltpu.make_async_remote_copy(
@@ -385,8 +400,11 @@
     @pl.when(i == sp - 1)
     def _():
         for a in range(spt):
-            for q in range(tp):
-                either(a, q, tail(a, q)[0].wait_send, None)
+            here, remote, _ = tail(a)
+            pl.when(jnp.logical_not(here))(remote.wait_send)
+
+    for q in range(tp):
+        pl.when(root & (q != j))(relay(q).wait_send)
     for k in range(sp):
         pl.when(i != k)(tot(k).wait_send)
     for s in range(steps):
@@ -433,6 +451,8 @@
             pltpu.VMEM((spt, heads, length), F32),
             pltpu.VMEM((8, LANES), F32),
             pltpu.VMEM((sp, 8, LANES), F32),
+            pltpu.VMEM((spt, heads, LANES), F32),
+            pltpu.VMEM((spt, PAIR, gcols, n_size), F32),
             pltpu.VMEM((steps, PAIR, gcols, n_size), BF16),
             pltpu.VMEM((steps, PAIR, gcols, n_size), BF16),
             pltpu.VMEM((steps, PAIR, gcols, n_size), BF16),
@@ -444,7 +464,7 @@
             pltpu.VMEM(conv_w.shape, F32),
             pltpu.VMEM((1, conv_w.shape[1]), F32),
             dma((spt,)), dma, dma((steps, 2)), dma((4,)), dma((2,)), dma((spt,)), dma((spt,)),
-            dma((spt, tp)), dma((1,)), dma((sp,)), dma((sp,)), dma((steps,)), dma((steps,)),
+            dma((spt,)), dma((1,)), dma((tp,)), dma((sp,)), dma((sp,)), dma((steps,)), dma((steps,)),
             dma((steps,)), dma((steps,)), dma((steps, PAIR)), dma((sp // 4 + 1, gl)),
         ],
         compiler_params=pltpu.CompilerParams(

time: 54.2 us -> 48.2 us (0.89)
  Pallas kernels: 50.4 us -> 44.5 us
    pallas_call x1, Pallas kernels: 50.4 us -> 44.5 us  [per_device(): pl.pallas_call(functools.partial(kernel, dims), out_shape=(jax.ShapeDtype...]
where the time goes in v3:
time: 48.2 us; the launch traced here: 47.9 us
  Pallas kernels  44.5 us (92%)
  local copies, waits for them, and re-layouts  2.83 us (6%)
  between operations  0.64 us (1%)
    pallas_call x1, Pallas kernels, per_device(): pl.pallas_call(functools.partial(kernel, dims), out_shape=(jax.ShapeDtype...  44.5 us
    unnamed x2, local copies, waits for them, and re-layouts  2.83 us

profile of v3, /device:TPU:5, one launch (start us, length us, event | category | flops | bytes accessed | tf_op | source)
XLA Modules:
  0.0 47.9 jit_solution(5977581478605197325)
XLA Ops:
  0.6 44.5 %shard_map.140 = (bf16[1,8,64,128]{3,2,1,0:T(8,128)(2,1)}, bf16[1,8,64]{2,1,0:T(8,128)(2,1)}) custom-call(bf16[2,384,2048]{2,1,0:T(8,128)(2,1)} %x_ref.1, bf16[1,2048]{1,0:T(2,128)(2,1)} %xn_ref.1, bf16[2048,2048]{1,0:T(8,128)(2,1)} %wx_ref.1, bf16[2048,1024]{1,0:T(8,128)(2,1)} %wb_ref.1, bf16[2048,1024]{1,0:T(8,128)(2,1)} %wc_ref.1, ...), custom_call_target="tpu_custom_call" | custom-call | tf_op jit(solution)/shard_map/pallas_call | solution.py:430
  45.1 1.6 %copy.17 = bf16[1,8,64,128]{3,2,1,0:T(8,128)(2,1)} copy(bf16[1,8,64,128]{3,2,1,0:T(8,128)(2,1)} %get-tuple-element.4) | data formatting | bytes 262144
  46.7 1.3 %copy.18 = bf16[1,8,64]{2,1,0:T(8,128)(2,1)} copy(bf16[1,8,64]{2,1,0:T(8,128)(2,1)} %get-tuple-element.5) | data formatting | bytes 2048

commit v4 on v3

--- a/solution.py
+++ b/solution.py
@@ -35,7 +35,7 @@
     x_ref, xn_ref, wx_ref, wb_ref, wc_ref, wdt_ref, wz_ref,
     cw_hbm, cb_hbm, dtb_ref, alog_ref, dskip_ref, ng_ref,
     state_ref, read_ref,
-    xs, wxs, wbs, wdts, wxn, wbn, wcn, wzn, nt, pre0, pre1, padded,
+    xs, wxs, wbs, wdts, wn, pre_n, nt, pre0, pre1, padded,
     wt, tot_out, tot_in, fcol, terms, a_out, a_in, mine, b_in, st_out, st_in, head_s, read_s, cw_ref, cb_ref,
     x_sem, wdt_sem, w_sem, new_sem, conv_sem, halo_send, halo_recv, tail_send, tail_recv, relay_send,
     tot_send, tot_recv, a_send, a_recv, b_send, b_recv, st_send, st_recv,
@@ -86,11 +86,13 @@
         ))
     vcol = pl.multiple_of(j * (hl * p_size), LANES)
     gcol = pl.multiple_of(j * (gl * n_size), LANES)
+    part = gl * n_size
+    vparts = hl * p_size // part
+    sources = [wx_ref.at[:, pl.ds(pl.multiple_of(vcol + c * part, LANES), part)] for c in range(vparts)]
+    sources += [wb_ref.at[:, pl.ds(gcol, part)], wc_ref.at[:, pl.ds(gcol, part)]]
+    sources += [wz_ref.at[:, pl.ds(c * part, part)] for c in range(vparts)]
     new_copies = [
-        pltpu.make_async_copy(wx_ref.at[:, pl.ds(vcol, hl * p_size)], wxn, new_sem.at[0]),
-        pltpu.make_async_copy(wb_ref.at[:, pl.ds(gcol, gl * n_size)], wbn, new_sem.at[1]),
-        pltpu.make_async_copy(wc_ref.at[:, pl.ds(gcol, gl * n_size)], wcn, new_sem.at[2]),
-        pltpu.make_async_copy(wz_ref, wzn, new_sem.at[3]),
+        pltpu.make_async_copy(src, wn.at[c], new_sem.at[c]) for c, src in enumerate(sources)
     ]
     conv_copies = [
         pltpu.make_async_copy(cw_hbm, cw_ref, conv_sem.at[0]),
@@ -164,20 +166,23 @@
             device_id={"sp": k, "tp": j}, device_id_type=MESH)
 
     tot_out[...] = jnp.zeros_like(tot_out)
-    for a in range(spt):
-        x_copies[a].wait()
+    def sizes_of(a, carry):
+        pltpu.make_async_copy(x_ref.at[a], xs.at[a, pl.ds(EDGE, length)], x_sem.at[a]).wait()
         raw = lax.dot_general(
             xs[a, EDGE:, :], wdts[...], (((1,), (1,)), ((), ())), preferred_element_type=F32)
         padded[:, 0:heads] = softplus(rounded(raw) + dtb_ref[...])
-        tot_out[a:a + 1, :] = jnp.sum(padded[...], axis=0, keepdims=True)
+        tot_out[pl.ds(a, 1), :] = jnp.sum(padded[...], axis=0, keepdims=True)
         sizes = padded[...].T[0:heads]
-        rest = jnp.zeros_like(sizes)
-        left = sizes
+        split, left = [], sizes
         for _ in range(3):
-            term = left.astype(BF16)
-            rest += jnp.dot(term, later, preferred_element_type=F32)
-            left = left - term.astype(F32)
+            split.append(left.astype(BF16))
+            left = left - split[-1].astype(F32)
+        parts = jnp.dot(jnp.concatenate(split, axis=0), later, preferred_element_type=F32)
+        rest = parts[0:heads] + parts[heads:2 * heads] + parts[2 * heads:3 * heads]
         wt[a] = jnp.exp(rates[:, 0:1] * rest) * sizes
+        return carry
+
+    lax.fori_loop(0, spt, sizes_of, 0)
     tot_in[i] = tot_out[...]
     for k in range(sp):
         pl.when(i != k)(tot(k).start)
@@ -199,14 +204,16 @@
         for a in range(spt):
             fcol[a] = column(jnp.exp(rate_row * beyond[a:a + 1, 0:heads]))
 
-    def a_copy(s):
+    def a_copy(s, gp):
         return pltpu.make_async_remote_copy(
-            src_ref=a_out.at[s], dst_ref=a_in.at[s], send_sem=a_send.at[s], recv_sem=a_recv.at[s],
+            src_ref=a_out.at[s, gp], dst_ref=a_in.at[s, gp],
+            send_sem=a_send.at[s, gp], recv_sem=a_recv.at[s, gp],
             device_id={"sp": partner, "tp": j}, device_id_type=MESH)
 
-    def b_copy(s):
+    def b_copy(s, gp):
         return pltpu.make_async_remote_copy(
-            src_ref=st_out.at[s], dst_ref=b_in.at[s], send_sem=b_send.at[s], recv_sem=b_recv.at[s],
+            src_ref=st_out.at[s, gp], dst_ref=b_in.at[s, gp],
+            send_sem=b_send.at[s, gp], recv_sem=b_recv.at[s, gp],
             device_id={"sp": sibling, "tp": j}, device_id_type=MESH)
 
     slot = jnp.where(direct & (lax.rem(m, 2) == 1), pairs, m // 2)
@@ -222,35 +229,36 @@
         ), pltpu.make_async_copy(src, dst, sem)
 
     def pass_on(s):
-        a_copy(s).wait_recv()
-
-        def add(*more):
-            for gp in range(PAIR):
+        def piece(gp, carry):
+            a_copy(s, gp).wait_recv()
+
+            def add(*more):
                 for r in range(0, gcols, LANES):
                     total = mine[s, gp, r:r + LANES, :].astype(F32)
                     for ref in more:
                         total += ref[s, gp, r:r + LANES, :].astype(F32)
                     st_out[s, gp, r:r + LANES, :] = total.astype(BF16)
 
-        @pl.when(near)
-        def _():
-            b_copy(s).wait_recv()
-            add(a_in, b_in)
-
-        @pl.when(jnp.logical_not(near))
-        def _():
-            add(a_in)
-
-        @pl.when(far)
-        def _():
-            b_copy(s).start()
-
-        @pl.when(jnp.logical_not(far))
-        def _():
-            for gp in range(PAIR):
+            @pl.when(near)
+            def _():
+                b_copy(s, gp).wait_recv()
+                add(a_in, b_in)
+
+            @pl.when(jnp.logical_not(near))
+            def _():
+                add(a_in)
+
+            pl.when(far)(b_copy(s, gp).start)
+
+            @pl.when(jnp.logical_not(far))
+            def _():
                 here, remote, local = state_copy(s, gp)
                 pl.when(jnp.logical_not(here))(remote.start)
                 pl.when(here)(local.start)
+
+            return carry
+
+        lax.fori_loop(0, PAIR, piece, 0)
 
     lag = jnp.where(near, 2, 1)
     for c in conv_copies:
@@ -311,7 +319,7 @@
                 first, second = (factors[a][h:h + 1] * terms[a, gp, span, :] for a in range(spt))
                 a_out[s, gp, span, :] = jnp.where(member == 0, second, first).astype(BF16)
                 mine[s, gp, span, :] = jnp.where(member == 0, first, second).astype(BF16)
-        a_copy(s).start()
+            a_copy(s, gp).start()
         pl.when(s >= lag)(lambda: pass_on(s - lag))
 
         @pl.when(root & (s == steps - 1))
@@ -330,20 +338,25 @@
     for c in new_copies:
         c.wait()
 
-    def new_conv(w_ref, start, width):
-        pre = rounded(jnp.dot(nt[...], w_ref[...], preferred_element_type=F32))
+    def new_rows(c, carry):
+        pre_n[c] = rounded(jnp.dot(nt[...], wn[c], preferred_element_type=F32))
+        return carry
+
+    lax.fori_loop(0, len(sources), new_rows, 0)
+
+    def new_conv(c, start):
         start = pl.multiple_of(start, LANES)
-        acc = cb_ref[:, pl.ds(start, width)]
-        w = cw_ref[:, pl.ds(start, width)]
+        acc = cb_ref[:, pl.ds(start, part)]
+        w = cw_ref[:, pl.ds(start, part)]
         for o in range(taps):
             at = EDGE - taps + 1 + o
-            acc = acc + w[o:o + 1] * pre[at:at + 1]
+            acc = acc + w[o:o + 1] * pre_n[c, at:at + 1, :]
         return rounded(silu(acc))
 
-    new_values = new_conv(wxn, vcol, hl * p_size)
-    new_keys = new_conv(wbn, inner + gcol, gl * n_size)
-    new_query = new_conv(wcn, inner + keys_all + gcol, gl * n_size)
-    gate = rounded(jnp.dot(newest, wzn[...], preferred_element_type=F32)[0:1])
+    new_values = jnp.concatenate([new_conv(c, vcol + c * part) for c in range(vparts)], axis=1)
+    new_keys = new_conv(vparts, inner + gcol)
+    new_query = new_conv(vparts + 1, inner + keys_all + gcol)
+    gate = jnp.concatenate([pre_n[vparts + 2 + c, EDGE:EDGE + 1, :] for c in range(vparts)], axis=1)
     new_raw = rounded(lax.dot_general(
         newest, wdts[...], (((1,), (1,)), ((), ())), preferred_element_type=F32)[0:1])
     new_steps = softplus(new_raw + dtb_ref[...])
@@ -408,9 +421,9 @@
     for k in range(sp):
         pl.when(i != k)(tot(k).wait_send)
     for s in range(steps):
-        a_copy(s).wait_send()
-        pl.when(far)(b_copy(s).wait_send)
         for gp in range(PAIR):
+            a_copy(s, gp).wait_send()
+            pl.when(far)(b_copy(s, gp).wait_send)
             here, remote, _ = state_copy(s, gp)
             pl.when(jnp.logical_not(far) & jnp.logical_not(here))(remote.wait_send)
 
@@ -424,6 +437,7 @@
     assert x_new.shape[0] == 1 and sp == spt * tp and spt == 2 and sp % 4 == 0
     steps, gcols = groups // PAIR, ratio * p_size
     tiles = PAIR * (gcols + n_size) // LANES
+    news = 2 + 2 * (hl * p_size) // (gl * n_size)
     any_spec = pl.BlockSpec(memory_space=pl.ANY)
     vmem = pl.BlockSpec(memory_space=pltpu.VMEM)
     dma = pltpu.SemaphoreType.DMA
@@ -440,10 +454,8 @@
             pltpu.VMEM((steps, width, PAIR * gcols), BF16),
             pltpu.VMEM((steps, width, PAIR * n_size), BF16),
             pltpu.VMEM((heads, width), BF16),
-            pltpu.VMEM((width, hl * p_size), BF16),
-            pltpu.VMEM((width, gl * n_size), BF16),
-            pltpu.VMEM((width, gl * n_size), BF16),
-            pltpu.VMEM((width, hl * p_size), BF16),
+            pltpu.VMEM((news, width, gl * n_size), BF16),
+            pltpu.VMEM((news, 2 * EDGE, gl * n_size), F32),
             pltpu.VMEM((2 * EDGE, width), BF16),
             pltpu.VMEM((tiles, EDGE + length, LANES), F32),
             pltpu.VMEM((tiles, EDGE + length, LANES), F32),
@@ -463,9 +475,9 @@
             pltpu.VMEM((hl, p_size), F32),
             pltpu.VMEM(conv_w.shape, F32),
             pltpu.VMEM((1, conv_w.shape[1]), F32),
-            dma((spt,)), dma, dma((steps, 2)), dma((4,)), dma((2,)), dma((spt,)), dma((spt,)),
-            dma((spt,)), dma((1,)), dma((tp,)), dma((sp,)), dma((sp,)), dma((steps,)), dma((steps,)),
-            dma((steps,)), dma((steps,)), dma((steps, PAIR)), dma((sp // 4 + 1, gl)),
+            dma((spt,)), dma, dma((steps, 2)), dma((news,)), dma((2,)), dma((spt,)), dma((spt,)),
+            dma((spt,)), dma((1,)), dma((tp,)), dma((sp,)), dma((sp,)), dma((steps, PAIR)), dma((steps, PAIR)),
+            dma((steps, PAIR)), dma((steps, PAIR)), dma((steps, PAIR)), dma((sp // 4 + 1, gl)),
         ],
         compiler_params=pltpu.CompilerParams(
             collective_id=0, has_side_effects=True, vmem_limit_bytes=60 * 1024 * 1024

time: 48.2 us -> 48.4 us (level)
  the two profiles are of different devices: /device:TPU:5 before, /device:TPU:23 now
where the time goes in v4:
time: 48.4 us; the launch traced here: 48.1 us
  Pallas kernels  44.7 us (92%)
  local copies, waits for them, and re-layouts  2.83 us (6%)
  between operations  0.64 us (1%)
    pallas_call x1, Pallas kernels, per_device(): pl.pallas_call(functools.partial(kernel, dims), out_shape=(jax.ShapeDtype...  44.7 us
    unnamed x2, local copies, waits for them, and re-layouts  2.83 us

profile of v4, /device:TPU:23, one launch (start us, length us, event | category | flops | bytes accessed | tf_op | source)
XLA Modules:
  0.0 48.1 jit_solution(6045852695344747152)
XLA Ops:
  0.6 44.7 %shard_map.140 = (bf16[1,8,64,128]{3,2,1,0:T(8,128)(2,1)}, bf16[1,8,64]{2,1,0:T(8,128)(2,1)}) custom-call(bf16[2,384,2048]{2,1,0:T(8,128)(2,1)} %x_ref.1, bf16[1,2048]{1,0:T(2,128)(2,1)} %xn_ref.1, bf16[2048,2048]{1,0:T(8,128)(2,1)} %wx_ref.1, bf16[2048,1024]{1,0:T(8,128)(2,1)} %wb_ref.1, bf16[2048,1024]{1,0:T(8,128)(2,1)} %wc_ref.1, ...), custom_call_target="tpu_custom_call" | custom-call | tf_op jit(solution)/shard_map/pallas_call | solution.py:444
  45.3 1.6 %copy.17 = bf16[1,8,64,128]{3,2,1,0:T(8,128)(2,1)} copy(bf16[1,8,64,128]{3,2,1,0:T(8,128)(2,1)} %get-tuple-element.4) | data formatting | bytes 262144
  46.9 1.3 %copy.18 = bf16[1,8,64]{2,1,0:T(8,128)(2,1)} copy(bf16[1,8,64]{2,1,0:T(8,128)(2,1)} %get-tuple-element.5) | data formatting | bytes 2048

commit v5 on v3

--- a/solution.py
+++ b/solution.py
@@ -415,6 +415,11 @@
             pl.when(jnp.logical_not(far) & jnp.logical_not(here))(remote.wait_send)
 
 
+def hand_over(state_in, read_in, state_out, read_out):
+    state_out[...] = state_in[...]
+    read_out[...] = read_in[...]
+
+
 def per_device(
     dims, x_in, x_new, w_x, w_b, w_c, w_dt, w_z, conv_w, conv_b, dt_bias, a_log, d_skip, norm_g
 ):
@@ -427,7 +432,7 @@
     any_spec = pl.BlockSpec(memory_space=pl.ANY)
     vmem = pl.BlockSpec(memory_space=pltpu.VMEM)
     dma = pltpu.SemaphoreType.DMA
-    return pl.pallas_call(
+    results = pl.pallas_call(
         functools.partial(kernel, dims),
         out_shape=(
             jax.ShapeDtypeStruct((1, hl, p_size, n_size), BF16),
@@ -474,6 +479,13 @@
         x_in, x_new, w_x, w_b, w_c, w_dt.T, w_z, conv_w, conv_b.reshape(1, -1),
         dt_bias.reshape(1, -1), a_log.reshape(1, -1), d_skip.reshape(1, -1), norm_g,
     )
+    return pl.pallas_call(
+        hand_over,
+        out_shape=tuple(jax.ShapeDtypeStruct(r.shape, r.dtype) for r in results),
+        in_specs=[vmem, vmem],
+        out_specs=(vmem, vmem),
+        compiler_params=pltpu.CompilerParams(vmem_limit_bytes=4 * 1024 * 1024),
+    )(*results)
 
 
 def solution(mesh):

time: 48.2 us -> 47.6 us (0.988)
  local copies, waits for them, and re-layouts: 2.83 us -> 1.56 us
  Pallas kernels: 44.5 us -> 45.1 us
    unnamed x2 -> x4, local copies, waits for them, and re-layouts: 2.83 us -> 1.56 us
    pallas_call x0 -> x1, Pallas kernels: none -> 0.67 us  [per_device(): pl.pallas_call(hand_over, out_shape=tuple((jax.ShapeDtypeStruct(r.shape,...]
where the time goes in v5:
time: 47.6 us; the launch traced here: 47.3 us
  Pallas kernels  45.1 us (95%)
  local copies, waits for them, and re-layouts  1.56 us (3%)
  between operations  0.65 us (1%)
    pallas_call x1, Pallas kernels, per_device(): pl.pallas_call(functools.partial(kernel, dims), out_shape=(jax.ShapeDtype...  44.5 us
    unnamed x4, local copies, waits for them, and re-layouts  1.56 us

profile of v5, /device:TPU:5, one launch (start us, length us, event | category | flops | bytes accessed | tf_op | source)
XLA Modules:
  0.0 47.3 jit_solution(12457913090043972994)
XLA Ops:
  0.6 44.5 %shard_map.140 = (bf16[1,8,64,128]{3,2,1,0:T(8,128)(2,1)}, bf16[1,8,64]{2,1,0:T(8,128)(2,1)}) custom-call(bf16[2,384,2048]{2,1,0:T(8,128)(2,1)} %x_ref.1, bf16[1,2048]{1,0:T(2,128)(2,1)} %xn_ref.1, bf16[2048,2048]{1,0:T(8,128)(2,1)} %wx_ref.1, bf16[2048,1024]{1,0:T(8,128)(2,1)} %wb_ref.1, bf16[2048,1024]{1,0:T(8,128)(2,1)} %wc_ref.1, ...), custom_call_target="tpu_custom_call" | custom-call | tf_op jit(solution)/shard_map/pallas_call | solution.py:435
  45.1 0.0 copy-start
  45.1 0.9 %copy-done = bf16[1,8,64,128]{3,2,1,0:T(8,128)(2,1)S(1)} copy-done((bf16[1,8,64,128]{3,2,1,0:T(8,128)(2,1)S(1)}, bf16[1,8,64,128]{3,2,1,0:T(8,128)(2,1)}, u32[]{:S(2)}) %copy-start) | copy-done | bytes 131096
  46.0 0.0 copy-start.1
  46.0 0.7 %copy-done.1 = bf16[1,8,64]{2,1,0:T(8,128)(2,1)S(1)} copy-done((bf16[1,8,64]{2,1,0:T(8,128)(2,1)S(1)}, bf16[1,8,64]{2,1,0:T(8,128)(2,1)}, u32[]{:S(2)}) %copy-start.1) | copy-done | bytes 1048
  46.7 0.7 %shard_map.141 = (bf16[1,8,64,128]{3,2,1,0:T(8,128)(2,1)}, bf16[1,8,64]{2,1,0:T(8,128)(2,1)}) custom-call(bf16[1,8,64,128]{3,2,1,0:T(8,128)(2,1)S(1)} %copy-done, bf16[1,8,64]{2,1,0:T(8,128)(2,1)S(1)} %copy-done.1), custom_call_target="tpu_custom_call" | custom-call | tf_op jit(solution)/shard_map/pallas_call | solution.py:482
Async XLA Ops:
  45.1 0.9 %copy-start = (bf16[1,8,64,128]{3,2,1,0:T(8,128)(2,1)S(1)}, bf16[1,8,64,128]{3,2,1,0:T(8,128)(2,1)}, u32[]{:S(2)}) copy-start(bf16[1,8,64,128]{3,2,1,0:T(8,128)(2,1)} %get-tuple-element.4.state_in) | copy-start | bytes 393220
  46.0 0.7 %copy-start.1 = (bf16[1,8,64]{2,1,0:T(8,128)(2,1)S(1)}, bf16[1,8,64]{2,1,0:T(8,128)(2,1)}, u32[]{:S(2)}) copy-start(bf16[1,8,64]{2,1,0:T(8,128)(2,1)} %get-tuple-element.5.read_in) | copy-start | bytes 3076
